TPU v7x, 256 devices: a whole 4x4x8 slice. The times are simulated.
256 devices in a mesh: kv: 16 (over y, x), tp: 16 (over z, core).
Axes of the slice: x: 4, y: 4, z: 8, core: 2. Of those that a mesh axis runs over, the one named last changes fastest.
Arguments:
- tokens: bfloat16 [1024, 4096], P('tp', 'kv'), may hold values from -19 to 19, as said below
- lengths: int32 [1024], P('kv'), may hold values from 1 to 16384, 4194304 in all
- state_block: float32 [1024, 64, 2048], P('kv', None, 'tp'), may hold values from -6 to 6
- cached_keys: bfloat16 [1024, 128, 2048], P('kv', None, 'tp'), may hold values from -0.75 to 0.75
- cached_values: bfloat16 [1024, 128, 2048], P('kv', None, 'tp'), may hold values from -6 to 6
- query_weight: bfloat16 [4096, 2048], P('kv', 'tp'), may hold values from -0.09375 to 0.09375
- key_weight: bfloat16 [4096, 2048], P('kv', 'tp'), may hold values from -0.09375 to 0.09375
- value_weight: bfloat16 [4096, 2048], P('kv', 'tp'), may hold values from -0.09375 to 0.09375
- gate_weight: bfloat16 [4096, 2048], P('kv', 'tp'), may hold values from -0.09375 to 0.09375
- decay_rate: float32 [32], P('tp'), may hold values from 0.0005 to 0.05
- head_gain: float32 [2048], P('tp'), may hold values from 0.1 to 1.9
- out_weight: bfloat16 [2048, 4096], P('tp', 'kv'), may hold values from -0.125 to 0.125
- mixer_gain: float32 [4096], P('kv'), may hold values from 0.1 to 1.9
- up_weight: bfloat16 [4096, 16384], P('kv', 'tp'), may hold values from -0.09375 to 0.09375
- down_weight: bfloat16 [16384, 4096], P('tp', 'kv'), may hold values from -0.046875 to 0.046875
- final_gain: float32 [4096], P('kv'), may hold values from 0.1 to 1.9
Outputs:
- next_rows: bfloat16 [1024, 4096], P('tp', 'kv')
Inputs may be any that keep to these rules, and one draw needn't show every extreme that they name: `tokens`: the rows' column groups have scales that differ between groups.
All inputs are finite; a program needn't handle non-finite values. No bound on the sum of `lengths` on one device may be relied on, other than what follows from the above.
Results may differ from a plain program's by a relative error of at most 0.0095.
Values may be sent and summed in bfloat16 or wider, within the bound.
A program may use at most 64 MiB of HBM per device.

v0:
```python
import functools

import jax
import jax.numpy as jnp
from jax import lax
from jax.sharding import Mesh
from jax.sharding import PartitionSpec as P

HDIM = 64
BLK = 128
KV = ("kv_0", "kv_1")


ALPHA = 2.0**0.5
EPS = 1e-05


def by_axis(x, axes):
    return functools.reduce(lax.psum, axes, x)


def copy_for_each(x, axis):
    peers = lax.axis_size(axis)
    return lax.all_to_all(jnp.broadcast_to(x[None], (peers, *x.shape)), axis, 0, 0, tiled=True)


def joined_along(parts, dim):
    parts = jnp.moveaxis(parts, 0, dim)
    dims = parts.shape
    return parts.reshape(*dims[:dim], dims[dim] * dims[dim + 1], *dims[dim + 2 :])


def gather_directly(x, axis, dim):
    parts = copy_for_each(x, axis)
    return joined_along(parts, dim)


def split_up(x, dim, peers):
    dims = x.shape
    parts = x.reshape(*dims[:dim], peers, dims[dim] // peers, *dims[dim + 1 :])
    return jnp.moveaxis(parts, dim, 0)


def sent_and_summed(x, axis, dim):
    parts = split_up(x, dim, lax.axis_size(axis))
    arrived = lax.all_to_all(parts, axis, split_axis=0, concat_axis=0, tiled=True)
    return arrived.sum(axis=0)


def rotate(vectors, positions):
    half = vectors.shape[-1] // 2
    inverse = 10000.0 ** (-jnp.arange(half, dtype=jnp.float32) / half)
    angle = positions.astype(jnp.float32)[:, None] * inverse[None, :]
    cosine = jnp.cos(angle)[:, None, :]
    sine = jnp.sin(angle)[:, None, :]
    former, latter = (vectors[..., :half], vectors[..., half:])
    return jnp.concatenate([former * cosine - latter * sine, latter * cosine + former * sine], -1)


def normalize(values, gain):
    width = values.shape[1] * lax.axis_size(KV)
    total, square = (by_axis(jnp.sum(values, 1), KV), by_axis(jnp.sum(values * values, 1), KV))
    mean = total / width
    centred = values - mean[:, None]
    spread = square / width - mean * mean
    return centred * lax.rsqrt(spread[:, None] + EPS) * gain[None, :]


def retain(query, keyed, valued, gated, lengths, state, keys, values, rate, gain):
    count = query.shape[0]
    heads = rate.shape[0]
    q_rot = rotate(query.astype(jnp.float32).reshape(count, heads, HDIM), lengths).astype(
        jnp.bfloat16
    )
    k_rot = (rotate(keyed.astype(jnp.float32).reshape(count, heads, HDIM), lengths) * 0.125).astype(
        jnp.bfloat16
    )
    v_new = valued.astype(jnp.float32).reshape(count, heads, HDIM)
    cached_k = keys.reshape(count, BLK, heads, HDIM)
    cached_v = values.reshape(count, BLK, heads, HDIM)
    scores = jnp.einsum("shn,sihn->shi", q_rot, cached_k, preferred_element_type=jnp.float32)
    offset = lengths % BLK
    slots = jnp.arange(BLK, dtype=jnp.int32)
    lag = jnp.maximum(offset[:, None] - slots[None, :], 0).astype(jnp.float32)
    live = (slots[None, :] < offset[:, None])[:, None, :]
    factor = jnp.where(live, jnp.exp(-rate[None, :, None] * lag[:, None, :]), 0.0)
    weights = (scores * factor).astype(jnp.bfloat16)
    own = jnp.einsum("shn,shn->sh", q_rot, k_rot, preferred_element_type=jnp.float32).astype(
        jnp.bfloat16
    )
    inner = jnp.einsum("shi,sihn->shn", weights, cached_v, preferred_element_type=jnp.float32)
    inner = inner + own.astype(jnp.float32)[..., None] * v_new
    carried = jnp.exp(-rate[None, :] * (offset[:, None] + 1).astype(jnp.float32))
    cross = (
        jnp.einsum(
            "shk,skhv->shv", q_rot.astype(jnp.float32), state.reshape(count, HDIM, heads, HDIM)
        )
        * carried[..., None]
    )
    retained = inner + cross
    mean = jnp.mean(retained, -1, keepdims=True)
    centred = retained - mean
    spread = jnp.mean(centred * centred, -1, keepdims=True)
    normed = centred * lax.rsqrt(spread + EPS) * gain.reshape(heads, HDIM)[None]
    gate_f = jax.nn.silu(gated.astype(jnp.float32).reshape(count, heads, HDIM))
    return (gate_f * normed).reshape(count, heads * HDIM).astype(jnp.bfloat16)


def per_device(
    tokens,
    lengths,
    state_block,
    cached_keys,
    cached_values,
    query_weight,
    key_weight,
    value_weight,
    gate_weight,
    decay_rate,
    head_gain,
    out_weight,
    mixer_gain,
    up_weight,
    down_weight,
    final_gain,
):
    all_rows = gather_directly(tokens, "tp", 0)
    width = query_weight.shape[1]
    piece = all_rows
    summed = sent_and_summed(
        jnp.concatenate(
            [
                jnp.dot(piece, weight, preferred_element_type=jnp.float32)
                for weight in (query_weight, key_weight, value_weight, gate_weight)
            ],
            1,
        ),
        KV,
        0,
    ).astype(jnp.bfloat16)
    query, keyed, valued, gated = [
        summed[:, index * width : (index + 1) * width] for index in range(4)
    ]
    mixed = retain(
        query,
        keyed,
        valued,
        gated,
        lengths,
        state_block,
        cached_keys,
        cached_values,
        decay_rate,
        head_gain,
    )
    mixed_all = gather_directly(mixed, KV, 0)
    piece = mixed_all
    branch = sent_and_summed(
        jnp.dot(piece, out_weight, preferred_element_type=jnp.float32), "tp", 0
    )
    hidden = normalize(ALPHA * tokens.astype(jnp.float32) + branch, mixer_gain).astype(jnp.bfloat16)
    hidden_all = gather_directly(hidden, "tp", 0)
    piece = hidden_all
    upward = sent_and_summed(jnp.dot(piece, up_weight, preferred_element_type=jnp.float32), KV, 0)
    active = jnp.square(jax.nn.relu(upward)).astype(jnp.bfloat16)
    terms = jnp.dot(gather_directly(active, KV, 0), down_weight, preferred_element_type=jnp.float32)
    downward = sent_and_summed(terms, "tp", 0)
    result = normalize(ALPHA * hidden.astype(jnp.float32) + downward, final_gain)
    return result.astype(jnp.bfloat16)


def solution(mesh):
    finer = Mesh(mesh.devices.reshape(4, 4, mesh.shape["tp"]), ("kv_0", "kv_1", "tp"))
    placed = (
        P("tp", KV),
        P(KV),
        P(KV, None, "tp"),
        P(KV, None, "tp"),
        P(KV, None, "tp"),
        P(KV, "tp"),
        P(KV, "tp"),
        P(KV, "tp"),
        P(KV, "tp"),
        P("tp"),
        P("tp"),
        P("tp", KV),
        P(KV),
        P(KV, "tp"),
        P("tp", KV),
        P(KV),
    )
    return jax.shard_map(
        per_device, mesh=finer, in_specs=placed, out_specs=P("tp", KV), check_vma=False
    )
```

profile of v0, /device:TPU:2, one launch (start us, length us, event | category | flops | bytes accessed | tf_op | source)
XLA Modules:
  0.0 297.4 jit_solution(9212659954619305765)
XLA Ops:
  0.0 0.9 broadcast_in_dim.16
  0.9 0.0 copy-start.7
  0.9 24.4 %all_to_all.40 = bf16[16,64,256]{2,1,0:T(8,128)(2,1)S(1)} all-to-all(bf16[16,64,256]{2,1,0:T(8,128)(2,1)S(1)} %broadcast_in_dim.16), channel_id=1, replica_groups=mesh['kv_0'=4,'kv_1'=4,'tp'=16] {'tp'}, dimensions={0} | all-to-all | bytes 1048576 | tf_op jit(solution)/shard_map/all_to_all | solution.py:24
  25.3 1.1 fusion.26
  26.5 0.3 fusion.25
  26.8 0.3 fusion.24
  27.1 0.0 copy-done.7
  27.1 0.3 fusion.23
  27.5 0.1 pad_maximum_fusion
  27.6 1.9 copy.23
  29.5 7.6 %all-to-all-start.1 = ((f32[16,64,512]{2,1,0:T(8,128)}), f32[16,64,512]{2,1,0:T(8,128)S(1)}, u32[]{:S(2)}, u32[]{:S(2)}) async-start(f32[16,64,512]{2,1,0:T(8,128)} %bitcast.40), calls=%async_computation.1 | async-start | bytes 4194304 | tf_op jit(solution)/shard_map/all_to_all | solution.py:46
  37.1 0.1 mul.243
  37.2 0.1 multiply_exponential_fusion
  37.3 0.1 copy.26
  37.4 5.1 %reshape.219 = bf16[64,64,2,64]{3,2,1,0:T(2,128)(2,1)} reshape(f32[64,64,128]{2,1,0:T(8,128)} %param.18) | data formatting | bytes 3145728 | tf_op jit(solution)/shard_map/reshape | solution.py:96
  42.5 4.1 %copy.24 = bf16[64,128,128]{1,2,0:T(8,128)(2,1)} copy(bf16[64,128,128]{2,1,0:T(8,128)(2,1)} %param.19) | data formatting | bytes 4194304 | tf_op args[3]
  46.6 4.1 %copy.25 = bf16[64,128,128]{1,2,0:T(8,128)(2,1)} copy(bf16[64,128,128]{2,1,0:T(8,128)(2,1)} %param.20) | data formatting | bytes 4194304 | tf_op args[4]
  50.7 0.1 iota_compare_fusion
  50.8 0.1 maximum_convert_fusion
  50.9 0.2 multiply_cosine_fusion
  51.1 16.0 %all-to-all-done.1 = f32[16,64,512]{2,1,0:T(8,128)S(1)} async-done(((f32[16,64,512]{2,1,0:T(8,128)}), f32[16,64,512]{2,1,0:T(8,128)S(1)}, u32[]{:S(2)}, u32[]{:S(2)}) %all-to-all-start.1) | async-done | bytes 2097184 | tf_op jit(solution)/shard_map/all_to_all | solution.py:46
  67.1 0.2 reduce_sum.90
  67.2 0.0 copy-start.2
  67.3 0.1 reshape.225
  67.4 0.1 reshape.223
  67.5 0.2 multiply_subtract_fusion
  67.7 0.1 fusion.21
  67.8 0.3 fusion.10
  68.1 0.1 reshape.221
  68.2 0.1 reshape.227
  68.4 2.4 fusion
  70.7 0.0 copy-done.2
  70.7 0.7 fusion.15
  71.4 0.1 fusion.17
  71.6 1.2 fusion.11
  72.7 0.3 fusion.22
  73.1 0.2 multiply_reduce_fusion.2
  73.3 0.2 fusion.13
  73.5 0.1 convert_element_type.75
  73.7 16.0 %all_to_all.41 = bf16[16,64,128]{2,1,0:T(8,128)(2,1)S(1)} all-to-all(bf16[16,64,128]{2,1,0:T(8,128)(2,1)S(1)} %broadcast_in_dim.19), channel_id=1, replica_groups=mesh['kv_0'=4,'kv_1'=4,'tp'=16] {'kv_0','kv_1'}, dimensions={0} | all-to-all | bytes 524288 | tf_op jit(solution)/shard_map/all_to_all | solution.py:24
  89.6 0.0 copy-done.8
  89.6 0.3 fusion.8
  89.9 29.8 %all_to_all.42 = f32[16,64,256]{2,1,0:T(8,128)S(1)} all-to-all(f32[16,64,256]{2,1,0:T(8,128)S(1)} %fusion.8), channel_id=1, replica_groups=mesh['kv_0'=4,'kv_1'=4,'tp'=16] {'tp'}, dimensions={0} | all-to-all | bytes 2097152 | tf_op jit(solution)/shard_map/all_to_all | solution.py:46
  119.7 0.1 reduce_sum.93
  119.8 0.1 fusion.18
  119.9 8.6 %all-reduce.3 = (f32[64]{0:T(128)S(1)}, f32[64]{0:T(128)S(1)}) all-reduce(f32[64]{0:T(128)S(1)} %get-tuple-element.8, f32[64]{0:T(128)S(1)} %get-tuple-element.7), channel_id=1, replica_groups=mesh['kv_0'=4,'kv_1'=4,'tp'=16] {'kv_0'}, use_global_device_ids=true, to_apply=%region_8.9 | all-reduce | flops 128 | bytes 1024 | tf_op jit(solution)/shard_map/psum | solution.py:19
  128.5 9.2 %all-reduce.1 = (f32[64]{0:T(128)S(1)}, f32[64]{0:T(128)S(1)}) all-reduce(f32[64]{0:T(128)S(1)} %get-tuple-element.15, f32[64]{0:T(128)S(1)} %get-tuple-element.16), channel_id=1, replica_groups=mesh['kv_0'=4,'kv_1'=4,'tp'=16] {'kv_1'}, use_global_device_ids=true, to_apply=%region_9.10 | all-reduce | flops 128 | bytes 1024 | tf_op jit(solution)/shard_map/psum | solution.py:19
  137.7 0.1 multiply_convert_fusion.2
  137.8 20.0 %all_to_all.43 = bf16[16,64,256]{2,1,0:T(8,128)(2,1)S(1)} all-to-all(bf16[16,64,256]{2,1,0:T(8,128)(2,1)S(1)} %broadcast_in_dim.20), channel_id=1, replica_groups=mesh['kv_0'=4,'kv_1'=4,'tp'=16] {'tp'}, dimensions={0} | all-to-all | bytes 1048576 | tf_op jit(solution)/shard_map/all_to_all | solution.py:24
  157.8 0.0 copy-done
  157.8 0.7 fusion.4
  158.5 54.7 %all_to_all.44 = f32[16,64,1024]{2,1,0:T(8,128)} all-to-all(f32[16,64,1024]{2,1,0:T(8,128)S(1)} %fusion.4), channel_id=1, replica_groups=mesh['kv_0'=4,'kv_1'=4,'tp'=16] {'kv_0','kv_1'}, dimensions={0} | all-to-all | bytes 8388608 | tf_op jit(solution)/shard_map/all_to_all | solution.py:46
  213.2 2.5 reduce_sum.96
  215.7 0.3 broadcast_in_dim.21
  216.0 0.0 copy-start.3
  216.0 32.3 %all_to_all.45 = bf16[16,64,1024]{2,1,0:T(8,128)(2,1)S(1)} all-to-all(bf16[16,64,1024]{2,1,0:T(8,128)(2,1)S(1)} %broadcast_in_dim.21), channel_id=1, replica_groups=mesh['kv_0'=4,'kv_1'=4,'tp'=16] {'kv_0','kv_1'}, dimensions={0} | all-to-all | bytes 4194304 | tf_op jit(solution)/shard_map/all_to_all | solution.py:24
  248.3 0.7 fusion.2
  249.0 0.0 copy-start.10
  249.0 29.8 %all_to_all.46 = f32[16,64,256]{2,1,0:T(8,128)S(1)} all-to-all(f32[16,64,256]{2,1,0:T(8,128)S(1)} %fusion.2), channel_id=1, replica_groups=mesh['kv_0'=4,'kv_1'=4,'tp'=16] {'tp'}, dimensions={0} | all-to-all | bytes 2097152 | tf_op jit(solution)/shard_map/all_to_all | solution.py:46
  278.8 0.1 reduce_sum.97
  278.9 0.1 fusion.19
  279.0 8.6 %all-reduce.2 = (f32[64]{0:T(128)S(1)}, f32[64]{0:T(128)S(1)}) all-reduce(f32[64]{0:T(128)S(1)} %get-tuple-element.6, f32[64]{0:T(128)S(1)} %get-tuple-element.5), channel_id=1, replica_groups=mesh['kv_0'=4,'kv_1'=4,'tp'=16] {'kv_0'}, use_global_device_ids=true, to_apply=%region_16.17 | all-reduce | flops 128 | bytes 1024 | tf_op jit(solution)/shard_map/psum | solution.py:19
  287.5 9.2 %all-reduce = (f32[64]{0:T(128)S(1)}, f32[64]{0:T(128)S(1)}) all-reduce(f32[64]{0:T(128)S(1)} %get-tuple-element.13, f32[64]{0:T(128)S(1)} %get-tuple-element.14), channel_id=1, replica_groups=mesh['kv_0'=4,'kv_1'=4,'tp'=16] {'kv_1'}, use_global_device_ids=true, to_apply=%region_17.18 | all-reduce | flops 128 | bytes 1024 | tf_op jit(solution)/shard_map/psum | solution.py:19
  296.7 0.7 multiply_convert_fusion.1
  (32 shorter events, 0.2 us)
Async XLA Ops:
  0.0 157.8 %copy-start = (bf16[256,1024]{1,0:T(8,128)(2,1)S(1)}, bf16[256,1024]{1,0:T(8,128)(2,1)}, u32[]{:S(2)}) copy-start(bf16[256,1024]{1,0:T(8,128)(2,1)} %param.29) | copy-start | bytes 1572868
  0.0 26.5 %copy-start.5 = (bf16[256,128]{1,0:T(8,128)(2,1)S(1)}, bf16[256,128]{1,0:T(8,128)(2,1)}, u32[]{:S(2)}) copy-start(bf16[256,128]{1,0:T(8,128)(2,1)} %param.23) | copy-start | bytes 196612
  0.0 26.8 %copy-start.6 = (bf16[256,128]{1,0:T(8,128)(2,1)S(1)}, bf16[256,128]{1,0:T(8,128)(2,1)}, u32[]{:S(2)}) copy-start(bf16[256,128]{1,0:T(8,128)(2,1)} %param.22) | copy-start | bytes 196612
  0.9 26.2 %copy-start.7 = (bf16[256,128]{1,0:T(8,128)(2,1)S(1)}, bf16[256,128]{1,0:T(8,128)(2,1)}, u32[]{:S(2)}) copy-start(bf16[256,128]{1,0:T(8,128)(2,1)} %param.21) | copy-start | bytes 196612
  29.5 7.6 %copy-start.12 = (f32[2]{0:T(128)S(1)}, f32[2]{0:T(128)}, u32[]{:S(2)}) copy-start(f32[2]{0:T(128)} %param.25) | copy-start | bytes 28
  29.5 7.6 %copy-start.13 = (f32[128]{0:T(128)S(1)}, f32[128]{0:T(128)}, u32[]{:S(2)}) copy-start(f32[128]{0:T(128)} %param.26) | copy-start | bytes 1540
  29.5 7.7 %copy-start.11 = (s32[64]{0:T(128)S(1)}, s32[64]{0:T(128)}, u32[]{:S(2)}) copy-start(s32[64]{0:T(128)} %param.17) | copy-start | bytes 772
  29.5 37.6 %all-to-all-start.1 = ((f32[16,64,512]{2,1,0:T(8,128)}), f32[16,64,512]{2,1,0:T(8,128)S(1)}, u32[]{:S(2)}, u32[]{:S(2)}) async-start(f32[16,64,512]{2,1,0:T(8,128)} %bitcast.40), calls=%async_computation.1 | async-start | bytes 4194304 | tf_op jit(solution)/shard_map/all_to_all | solution.py:46
  67.2 3.5 %copy-start.2 = (bf16[64,128,128]{1,2,0:T(8,128)(2,1)S(1)}, bf16[64,128,128]{1,2,0:T(8,128)(2,1)}, u32[]{:S(2)}) copy-start(bf16[64,128,128]{1,2,0:T(8,128)(2,1)} %copy.24) | copy-start | bytes 6291460
  68.3 3.2 %copy-start.1 = (bf16[64,128,128]{1,2,0:T(8,128)(2,1)S(1)}, bf16[64,128,128]{1,2,0:T(8,128)(2,1)}, u32[]{:S(2)}) copy-start(bf16[64,128,128]{1,2,0:T(8,128)(2,1)} %copy.25) | copy-start | bytes 6291460
  71.4 18.2 %copy-start.8 = (bf16[128,256]{1,0:T(8,128)(2,1)S(1)}, bf16[128,256]{1,0:T(8,128)(2,1)}, u32[]{:S(2)}) copy-start(bf16[128,256]{1,0:T(8,128)(2,1)} %param.27) | copy-start | bytes 196612
  89.6 30.1 %copy-start.4 = (bf16[64,256]{1,0:T(8,128)(2,1)S(1)}, bf16[64,256]{1,0:T(8,128)(2,1)}, u32[]{:S(2)}) copy-start(bf16[64,256]{1,0:T(8,128)(2,1)} %param.16) | copy-start | bytes 98308
  89.6 48.0 %copy-start.9 = (f32[256]{0:T(256)S(1)}, f32[256]{0:T(256)}, u32[]{:S(2)}) copy-start(f32[256]{0:T(256)} %param.28) | copy-start | bytes 3076
  216.0 32.3 %copy-start.3 = (bf16[1024,256]{1,0:T(8,128)(2,1)S(1)}, bf16[1024,256]{1,0:T(8,128)(2,1)}, u32[]{:S(2)}) copy-start(bf16[1024,256]{1,0:T(8,128)(2,1)} %param.30) | copy-start | bytes 1572868
  249.0 47.7 %copy-start.10 = (f32[256]{0:T(256)S(1)}, f32[256]{0:T(256)}, u32[]{:S(2)}) copy-start(f32[256]{0:T(256)} %param.31) | copy-start | bytes 3076
where the time goes:
time: 298 us; the launch traced here: 297 us
  blocking collectives  242 us (81%)
  local copies, waits for them, and re-layouts  17.1 us (6%)
  waiting for transfers between devices  16 us (5%)
  matrix products  7.98 us (3%)
  starting transfers between devices  7.61 us (3%)
  other arithmetic  5.97 us (2%)
    all_to_all x3, blocking collectives, sent_and_summed(): lax.all_to_all(parts, axis, split_axis=0, concat_axis=0, tiled=True)  114 us
    all_to_all x4, blocking collectives, copy_for_each(): lax.all_to_all(jnp.broadcast_to(x[None], (peers, *x.shape)), axis, 0, 0,...  92.6 us
    psum x4, blocking collectives, by_axis(): return functools.reduce(lax.psum, axes, x)  35.5 us
    all_to_all x1, waiting for transfers between devices, sent_and_summed(): lax.all_to_all(parts, axis, split_axis=0, concat_axis=0, tiled=True)  16 us
    unnamed x30, local copies, waits for them, and re-layouts  8.22 us
    all_to_all x1, starting transfers between devices, sent_and_summed(): lax.all_to_all(parts, axis, split_axis=0, concat_axis=0, tiled=True)  7.61 us
  transfers between devices with their start and end apart: 1, of which 1 were waited for; matrix products, arithmetic and copies ran while one was open for 5% of the time, Pallas kernels for 0%

commit v1 on v0

--- a/solution.py
+++ b/solution.py
@@ -42,9 +42,9 @@
 
 
 def sent_and_summed(x, axis, dim):
-    parts = split_up(x, dim, lax.axis_size(axis))
+    parts = split_up(x, dim, lax.axis_size(axis)).astype(jnp.bfloat16)
     arrived = lax.all_to_all(parts, axis, split_axis=0, concat_axis=0, tiled=True)
-    return arrived.sum(axis=0)
+    return arrived.astype(jnp.float32).sum(axis=0)
 
 
 def rotate(vectors, positions):
@@ -59,7 +59,8 @@
 
 def normalize(values, gain):
     width = values.shape[1] * lax.axis_size(KV)
-    total, square = (by_axis(jnp.sum(values, 1), KV), by_axis(jnp.sum(values * values, 1), KV))
+    sums = jnp.stack([jnp.sum(values, 1), jnp.sum(values * values, 1)])
+    total, square = copy_for_each(sums, KV).sum(axis=0)
     mean = total / width
     centred = values - mean[:, None]
     spread = square / width - mean * mean

time: 298 us -> 226 us (0.76)
  blocking collectives: 242 us -> 156 us
  starting transfers between devices: 7.61 us -> 16 us
    all_to_all x3, blocking collectives: 114 us -> 69.6 us  [sent_and_summed(): lax.all_to_all(parts, axis, split_axis=0, concat_axis=0, tiled=True)]
    psum x4 -> x0, blocking collectives: 35.5 us -> none  [by_axis(): return functools.reduce(lax.psum, axes, x)]
    all_to_all x0 -> x1, waiting for transfers between devices: none -> 13.8 us  [copy_for_each(): lax.all_to_all(jnp.broadcast_to(x[None], (peers, *x.shape)), axis, 0, 0,...]
    all_to_all x1, waiting for transfers between devices: 16 us -> 3.01 us  [sent_and_summed(): lax.all_to_all(parts, axis, split_axis=0, concat_axis=0, tiled=True)]
    all_to_all x0 -> x1, starting transfers between devices: none -> 8.57 us  [copy_for_each(): lax.all_to_all(jnp.broadcast_to(x[None], (peers, *x.shape)), axis, 0, 0,...]
    all_to_all x4 -> x5, blocking collectives: 92.6 us -> 86.5 us  [copy_for_each(): lax.all_to_all(jnp.broadcast_to(x[None], (peers, *x.shape)), axis, 0, 0,...]
    unnamed x30 -> x28, local copies, waits for them, and re-layouts: 8.22 us -> 8.55 us
  transfers between devices with their start and end apart: 1 -> 2, of which waited for: 1 -> 2; matrix products, arithmetic and copies ran while one was open for 5% -> 7% of each run, Pallas kernels for 0% -> 0%
where the time goes in v1:
time: 226 us; the launch traced here: 223 us
  blocking collectives  156 us (69%)
  local copies, waits for them, and re-layouts  18.9 us (8%)
  waiting for transfers between devices  16.8 us (7%)
  starting transfers between devices  16 us (7%)
  matrix products  7.97 us (4%)
  other arithmetic  6.62 us (3%)
    all_to_all x5, blocking collectives, copy_for_each(): lax.all_to_all(jnp.broadcast_to(x[None], (peers, *x.shape)), axis, 0, 0,...  86.5 us
    all_to_all x3, blocking collectives, sent_and_summed(): lax.all_to_all(parts, axis, split_axis=0, concat_axis=0, tiled=True)  69.6 us
    all_to_all x1, waiting for transfers between devices, copy_for_each(): lax.all_to_all(jnp.broadcast_to(x[None], (peers, *x.shape)), axis, 0, 0,...  13.8 us
    all_to_all x1, starting transfers between devices, copy_for_each(): lax.all_to_all(jnp.broadcast_to(x[None], (peers, *x.shape)), axis, 0, 0,...  8.57 us
    unnamed x28, local copies, waits for them, and re-layouts  8.55 us
    all_to_all x1, starting transfers between devices, sent_and_summed(): lax.all_to_all(parts, axis, split_axis=0, concat_axis=0, tiled=True)  7.48 us
    reshape x1, local copies, waits for them, and re-layouts, retain(): state.reshape(count, HDIM, heads, HDIM)  5.17 us
  transfers between devices with their start and end apart: 2, of which 2 were waited for; matrix products, arithmetic and copies ran while one was open for 7% of the time, Pallas kernels for 0%

profile of v1, /device:TPU:2, one launch (start us, length us, event | category | flops | bytes accessed | tf_op | source)
XLA Modules:
  0.0 222.8 jit_solution(2097501136191466114)
XLA Ops:
  0.0 1.7 broadcast_in_dim.20
  1.7 8.6 %all-to-all-start = ((bf16[16,64,256]{2,1,0:T(8,128)(2,1)}), bf16[16,64,256]{2,1,0:T(8,128)(2,1)S(1)}, u32[]{:S(2)}, u32[]{:S(2)}) async-start(bf16[16,64,256]{2,1,0:T(8,128)(2,1)} %broadcast_in_dim.20), calls=%async_computation | async-start | bytes 1048576 | tf_op jit(solution)/shard_map/all_to_all | solution.py:24
  10.3 0.7 neg.20
  10.9 0.7 mul.251
  11.7 0.7 add_convert_fusion.1
  12.4 13.8 %all-to-all-done = bf16[16,64,256]{2,1,0:T(8,128)(2,1)S(1)} async-done(((bf16[16,64,256]{2,1,0:T(8,128)(2,1)}), bf16[16,64,256]{2,1,0:T(8,128)(2,1)S(1)}, u32[]{:S(2)}, u32[]{:S(2)}) %all-to-all-start) | async-done | bytes 524320 | tf_op jit(solution)/shard_map/all_to_all | solution.py:24
  26.2 1.1 convolution_convert_fusion.3
  27.4 0.3 convolution_convert_fusion.4
  27.7 0.3 convolution_convert_fusion.5
  28.0 0.3 convolution_convert_fusion.6
  28.3 0.1 pad_maximum_fusion
  28.4 1.4 copy.28
  29.8 7.5 %all-to-all-start.1 = ((bf16[16,64,512]{2,1,0:T(8,128)(2,1)}), bf16[16,64,512]{2,1,0:T(8,128)(2,1)S(1)}, u32[]{:S(2)}, u32[]{:S(2)}) async-start(bf16[16,64,512]{2,1,0:T(8,128)(2,1)} %bitcast.1), calls=%async_computation.1 | async-start | bytes 2097152 | tf_op jit(solution)/shard_map/all_to_all | solution.py:46
  37.2 0.1 multiply_exponential_fusion
  37.3 0.1 copy.31
  37.4 5.2 %reshape.257 = bf16[64,64,2,64]{3,2,1,0:T(2,128)(2,1)} reshape(f32[64,64,128]{2,1,0:T(8,128)} %param.18) | data formatting | bytes 3145728 | tf_op jit(solution)/shard_map/reshape | solution.py:97
  42.6 4.1 %copy.29 = bf16[64,128,128]{1,2,0:T(8,128)(2,1)} copy(bf16[64,128,128]{2,1,0:T(8,128)(2,1)} %param.19) | data formatting | bytes 4194304 | tf_op args[3]
  46.7 4.1 %copy.30 = bf16[64,128,128]{1,2,0:T(8,128)(2,1)} copy(bf16[64,128,128]{2,1,0:T(8,128)(2,1)} %param.20) | data formatting | bytes 4194304 | tf_op args[4]
  50.7 0.1 iota_compare_fusion
  50.8 0.1 maximum_convert_fusion
  50.9 0.2 multiply_cosine_fusion
  51.1 3.0 %all-to-all-done.1 = bf16[16,64,512]{2,1,0:T(8,128)(2,1)S(1)} async-done(((bf16[16,64,512]{2,1,0:T(8,128)(2,1)}), bf16[16,64,512]{2,1,0:T(8,128)(2,1)S(1)}, u32[]{:S(2)}, u32[]{:S(2)}) %all-to-all-start.1) | async-done | bytes 1048608 | tf_op jit(solution)/shard_map/all_to_all | solution.py:46
  54.1 0.1 reduce_sum.111
  54.3 0.1 reshape.263
  54.4 0.1 reshape.265
  54.5 0.1 reshape.261
  54.6 0.2 multiply_subtract_fusion
  54.9 0.1 fusion.22
  55.0 0.3 fusion.7
  55.3 0.1 reshape.259
  55.4 2.4 %fusion = f32[64,2,1,64]{3,2,1,0:T(1,128)S(1)} fusion(bf16[64,64,2,64]{3,2,1,0:T(2,128)(2,1)} %reshape.257, bf16[64,2,64,1]{2,1,0,3:T(2,128)(2,1)S(1)} %fusion.22), kind=kOutput, calls=%fused_computation | convolution fusion | flops 1048576 | bytes 1097728 | tf_op jit(solution)/shard_map/shk,skhv->shv/dot_general | solution.py:96
  57.8 0.7 fusion.12
  58.4 0.1 fusion.14
  58.6 1.2 fusion.8
  59.8 0.3 fusion.23
  60.1 0.2 multiply_reduce_fusion.2
  60.4 0.2 fusion.10
  60.6 0.1 convert_element_type.96
  60.7 13.6 %all_to_all.50 = bf16[16,64,128]{2,1,0:T(8,128)(2,1)S(1)} all-to-all(bf16[16,64,128]{2,1,0:T(8,128)(2,1)S(1)} %broadcast_in_dim.27), channel_id=1, replica_groups=mesh['kv_0'=4,'kv_1'=4,'tp'=16] {'kv_0','kv_1'}, dimensions={0} | all-to-all | bytes 524288 | tf_op jit(solution)/shard_map/all_to_all | solution.py:24
  74.3 0.3 convolution_convert_fusion.2
  74.6 18.6 %all_to_all.51 = bf16[16,64,256]{2,1,0:T(8,128)(2,1)S(1)} all-to-all(bf16[16,64,256]{2,1,0:T(8,128)(2,1)S(1)} %convolution_convert_fusion.2), channel_id=1, replica_groups=mesh['kv_0'=4,'kv_1'=4,'tp'=16] {'tp'}, dimensions={0} | all-to-all | bytes 1048576 | tf_op jit(solution)/shard_map/all_to_all | solution.py:46
  93.1 0.1 convert_reduce_fusion.2
  93.2 0.1 fusion.15
  93.4 0.1 reshape.280
  93.4 10.5 %all_to_all.52 = f32[16,1,128]{2,1,0:T(1,128)S(1)} all-to-all(f32[16,1,128]{2,1,0:T(1,128)S(1)} %reshape.280), channel_id=1, replica_groups=mesh['kv_0'=4,'kv_1'=4,'tp'=16] {'kv_0','kv_1'}, dimensions={0} | all-to-all | bytes 16384 | tf_op jit(solution)/shard_map/all_to_all | solution.py:24
  103.9 0.5 broadcast.212
  104.4 0.7 reduce.3
  105.1 0.1 reshape.281
  105.2 0.1 multiply_convert_fusion.2
  105.4 20.0 %all_to_all.53 = bf16[16,64,256]{2,1,0:T(8,128)(2,1)S(1)} all-to-all(bf16[16,64,256]{2,1,0:T(8,128)(2,1)S(1)} %broadcast_in_dim.29), channel_id=1, replica_groups=mesh['kv_0'=4,'kv_1'=4,'tp'=16] {'tp'}, dimensions={0} | all-to-all | bytes 1048576 | tf_op jit(solution)/shard_map/all_to_all | solution.py:24
  125.3 0.7 convolution_convert_fusion
  126.1 32.5 %all_to_all.54 = bf16[16,64,1024]{2,1,0:T(8,128)(2,1)S(1)} all-to-all(bf16[16,64,1024]{2,1,0:T(8,128)(2,1)S(1)} %convolution_convert_fusion), channel_id=1, replica_groups=mesh['kv_0'=4,'kv_1'=4,'tp'=16] {'kv_0','kv_1'}, dimensions={0} | all-to-all | bytes 4194304 | tf_op jit(solution)/shard_map/all_to_all | solution.py:46
  158.6 0.4 convert_reduce_fusion
  159.0 0.3 broadcast_in_dim.30
  159.3 32.0 %all_to_all.55 = bf16[16,64,1024]{2,1,0:T(8,128)(2,1)S(1)} all-to-all(bf16[16,64,1024]{2,1,0:T(8,128)(2,1)S(1)} %broadcast_in_dim.30), channel_id=1, replica_groups=mesh['kv_0'=4,'kv_1'=4,'tp'=16] {'kv_0','kv_1'}, dimensions={0} | all-to-all | bytes 4194304 | tf_op jit(solution)/shard_map/all_to_all | solution.py:24
  191.2 0.7 convolution_convert_fusion.1
  191.9 18.6 %all_to_all.56 = bf16[16,64,256]{2,1,0:T(8,128)(2,1)S(1)} all-to-all(bf16[16,64,256]{2,1,0:T(8,128)(2,1)S(1)} %convolution_convert_fusion.1), channel_id=1, replica_groups=mesh['kv_0'=4,'kv_1'=4,'tp'=16] {'tp'}, dimensions={0} | all-to-all | bytes 1048576 | tf_op jit(solution)/shard_map/all_to_all | solution.py:46
  210.5 0.1 convert_reduce_fusion.1
  210.6 0.1 fusion.16
  210.7 0.1 reshape.282
  210.8 10.5 %all_to_all.57 = f32[16,1,128]{2,1,0:T(1,128)S(1)} all-to-all(f32[16,1,128]{2,1,0:T(1,128)S(1)} %reshape.282), channel_id=1, replica_groups=mesh['kv_0'=4,'kv_1'=4,'tp'=16] {'kv_0','kv_1'}, dimensions={0} | all-to-all | bytes 16384 | tf_op jit(solution)/shard_map/all_to_all | solution.py:24
  221.3 0.7 reduce.4
  222.0 0.1 reshape.283
  222.1 0.7 multiply_convert_fusion.1
  (40 shorter events, 0.3 us)
Async XLA Ops:
  0.0 125.3 %copy-start = (bf16[256,1024]{1,0:T(8,128)(2,1)S(1)}, bf16[256,1024]{1,0:T(8,128)(2,1)}, u32[]{:S(2)}) copy-start(bf16[256,1024]{1,0:T(8,128)(2,1)} %param.29) | copy-start | bytes 1572868
  0.0 27.4 %copy-start.4 = (bf16[256,128]{1,0:T(8,128)(2,1)S(1)}, bf16[256,128]{1,0:T(8,128)(2,1)}, u32[]{:S(2)}) copy-start(bf16[256,128]{1,0:T(8,128)(2,1)} %param.23) | copy-start | bytes 196612
  0.0 27.7 %copy-start.5 = (bf16[256,128]{1,0:T(8,128)(2,1)S(1)}, bf16[256,128]{1,0:T(8,128)(2,1)}, u32[]{:S(2)}) copy-start(bf16[256,128]{1,0:T(8,128)(2,1)} %param.22) | copy-start | bytes 196612
  0.0 28.0 %copy-start.6 = (bf16[256,128]{1,0:T(8,128)(2,1)S(1)}, bf16[256,128]{1,0:T(8,128)(2,1)}, u32[]{:S(2)}) copy-start(bf16[256,128]{1,0:T(8,128)(2,1)} %param.21) | copy-start | bytes 196612
  1.7 24.5 %all-to-all-start = ((bf16[16,64,256]{2,1,0:T(8,128)(2,1)}), bf16[16,64,256]{2,1,0:T(8,128)(2,1)S(1)}, u32[]{:S(2)}, u32[]{:S(2)}) async-start(bf16[16,64,256]{2,1,0:T(8,128)(2,1)} %broadcast_in_dim.20), calls=%async_computation | async-start | bytes 1048576 | tf_op jit(solution)/shard_map/all_to_all | solution.py:24
  29.8 24.4 %all-to-all-start.1 = ((bf16[16,64,512]{2,1,0:T(8,128)(2,1)}), bf16[16,64,512]{2,1,0:T(8,128)(2,1)S(1)}, u32[]{:S(2)}, u32[]{:S(2)}) async-start(bf16[16,64,512]{2,1,0:T(8,128)(2,1)} %bitcast.1), calls=%async_computation.1 | async-start | bytes 2097152 | tf_op jit(solution)/shard_map/all_to_all | solution.py:46
  54.3 3.5 %copy-start.2 = (bf16[64,128,128]{1,2,0:T(8,128)(2,1)S(1)}, bf16[64,128,128]{1,2,0:T(8,128)(2,1)}, u32[]{:S(2)}) copy-start(bf16[64,128,128]{1,2,0:T(8,128)(2,1)} %copy.29) | copy-start | bytes 6291460
  55.4 3.2 %copy-start.1 = (bf16[64,128,128]{1,2,0:T(8,128)(2,1)S(1)}, bf16[64,128,128]{1,2,0:T(8,128)(2,1)}, u32[]{:S(2)}) copy-start(bf16[64,128,128]{1,2,0:T(8,128)(2,1)} %copy.30) | copy-start | bytes 6291460
  58.4 15.9 %copy-start.7 = (bf16[128,256]{1,0:T(8,128)(2,1)S(1)}, bf16[128,256]{1,0:T(8,128)(2,1)}, u32[]{:S(2)}) copy-start(bf16[128,256]{1,0:T(8,128)(2,1)} %param.27) | copy-start | bytes 196612
  59.8 33.4 %copy-start.3 = (bf16[64,256]{1,0:T(8,128)(2,1)S(1)}, bf16[64,256]{1,0:T(8,128)(2,1)}, u32[]{:S(2)}) copy-start(bf16[64,256]{1,0:T(8,128)(2,1)} %param.16) | copy-start | bytes 98308
  60.1 45.2 %copy-start.8 = (f32[256]{0:T(256)S(1)}, f32[256]{0:T(256)}, u32[]{:S(2)}) copy-start(f32[256]{0:T(256)} %param.28) | copy-start | bytes 3076
  159.2 32.0 %copy-start.10 = (bf16[1024,256]{1,0:T(8,128)(2,1)S(1)}, bf16[1024,256]{1,0:T(8,128)(2,1)}, u32[]{:S(2)}) copy-start(bf16[1024,256]{1,0:T(8,128)(2,1)} %param.30) | copy-start | bytes 1572868
  191.2 30.9 %copy-start.9 = (f32[256]{0:T(256)S(1)}, f32[256]{0:T(256)}, u32[]{:S(2)}) copy-start(f32[256]{0:T(256)} %param.31) | copy-start | bytes 3076

commit v2 on v0

v2 whole, which is shorter than its diff:
```python
import functools

import jax
import jax.numpy as jnp
from jax import lax
from jax.experimental import pallas as pl
from jax.experimental.pallas import tpu as pltpu
from jax.sharding import Mesh
from jax.sharding import PartitionSpec as P

HDIM = 64
BLK = 128
ALPHA = 2.0**0.5
EPS = 1e-05
AXES = ("y", "x", "z", "c")
NEAR = (0, 1, 7, 2, 6, 3, 5, 4)
F32 = jnp.float32
B16 = jnp.bfloat16


def dot(a, b):
    return jnp.dot(a, b, preferred_element_type=F32)


def split_dot(a, b, terms, left=True):
    total = None
    rest = a if left else b
    for _ in range(terms):
        part = rest.astype(B16)
        rest = rest - part.astype(F32)
        term = dot(part, b) if left else dot(a, part)
        total = term if total is None else total + term
    return total


def copy_to(src, dst, send, recv, device):
    return pltpu.make_async_remote_copy(
        src_ref=src,
        dst_ref=dst,
        send_sem=send,
        recv_sem=recv,
        device_id=device,
        device_id_type=pl.DeviceIdType.MESH,
    )


def kernel(
    tok, cosine, sine, offset, rate, head_gain, mixer_gain, final_gain,
    state_h, keys_h, values_h, wq_h, wk_h, wv_h, wg_h, wo_h, wu_h, wd_h,
    out,
    state, keys, values, factor, wp, wo, wu, wd,
    t_all, b_out, b_in, qkvg, retained, mixed, m_all, d_out, d_in,
    s_out, s_in, hidden, h_all, g1_out, g1_in, g2_out, g2_in, act_all, e_out, e_in, f_out, f_in,
    local, send, r_w, r_a, r_b, r_c, r_d, r_e, r_f, r_g1, r_g2, r_h1, r_h2, r_i, r_j,
):
    y, x, z, c = [lax.axis_index(name) for name in AXES]
    kv = y * 4 + x
    sibling = (y, x, z, 1 - c)
    row_of = lax.rem(x, 2)
    owner = row_of == c

    def arrived(dst, sem):
        copy_to(dst, dst, send.at[0], sem, sibling).wait_recv()

    here = []

    def fetch(src, dst):
        here.append(pltpu.make_async_copy(src, dst, local.at[len(here)]))
        here[-1].start()

    quarter = [wp.at[c, :, pl.ds(128 * i, 128)] for i in range(4)]
    for src, dst in zip((wq_h, wk_h, wv_h, wg_h), quarter):
        fetch(src, dst)
    fetch(wo_h, wo.at[c])
    fetch(wu_h, wu.at[c])
    fetch(wd_h, wd.at[c])
    fetch(keys_h, keys)
    fetch(values_h, values)
    fetch(state_h, state)

    barrier = pltpu.get_barrier_semaphore()
    greeted = 0
    for dy in range(4):
        for dx in range(4):
            for dc in range(2):
                if dy or dx or dc:
                    peer = (lax.rem(y + dy, 4), lax.rem(x + dx, 4), z, lax.rem(c + dc, 2))
                    pl.semaphore_signal(barrier, inc=1, device_id=peer, device_id_type=pl.DeviceIdType.MESH)
                    greeted += 1
    for dz in range(1, 8):
        peer = (y, x, lax.rem(z + dz, 8), c)
        pl.semaphore_signal(barrier, inc=1, device_id=peer, device_id_type=pl.DeviceIdType.MESH)
        greeted += 1

    def decay(i, carry):
        rows = pl.ds(pl.multiple_of(i * 8, 8), 8)
        off = offset[rows, :][:, None, :]
        slot = lax.broadcasted_iota(jnp.int32, (8, BLK, 128), 1).astype(F32)
        lag = jnp.maximum(off - slot, 0.0)
        factor[rows] = jnp.where(slot < off, jnp.exp(-rate[...][None] * lag), 0.0)
        return carry

    lax.fori_loop(0, 8, decay, 0)
    t_all[z] = tok[...]
    pl.semaphore_wait(barrier, greeted)

    a_sends = []
    for d in NEAR[1:]:
        a_sends.append(copy_to(tok, t_all.at[z], send.at[d], r_a.at[z], (y, x, lax.rem(z + d, 8), c)))
        a_sends[-1].start()
    w_sends = []
    for i, (src, dst) in enumerate(
        [*zip((wq_h, wk_h, wv_h, wg_h), quarter), (wo_h, wo.at[c]), (wu_h, wu.at[c]), (wd_h, wd.at[c])]
    ):
        w_sends.append(copy_to(src, dst, send.at[8 + i], r_w.at[i], sibling))
        w_sends[-1].start()
    theirs = [wp.at[1 - c, :, pl.ds(128 * i, 128)] for i in range(4)] + [w.at[1 - c] for w in (wo, wu, wd)]
    for i in range(4):
        here[i].wait()
        arrived(theirs[i], r_w.at[i])

    b_sends = []
    for d in NEAR:
        zp = lax.rem(z + 8 - d, 8)
        if d:
            arrived(t_all.at[zp], r_a.at[zp])
        block = 2 * zp + c
        rows = t_all[zp]
        for core in range(2):
            part = dot(rows, wp[core]).astype(B16)
            mine = jnp.logical_and(block == kv, c == core)
            b_out[zp, core] = part
            copy = copy_to(
                b_out.at[zp, core], b_in.at[kv], send.at[16 + d * 2 + core], r_b.at[kv],
                (block // 4, lax.rem(block, 4), z, core),
            )
            b_sends.append((jnp.logical_not(mine), copy))

            @pl.when(mine)
            def _():
                b_in[kv] = part

            @pl.when(jnp.logical_not(mine))
            def _():
                copy.start()

    for copy in a_sends + w_sends:
        copy.wait_send()

    def wait_projected(i, carry):
        @pl.when(jnp.logical_not(jnp.logical_and(i == kv, owner)))
        def _():
            arrived(b_in.at[i], r_b.at[i])

        return carry

    lax.fori_loop(0, 16, wait_projected, 0)
    qkvg[...] = b_in[0].astype(F32)

    def add_projected(i, carry):
        qkvg[...] += b_in[i].astype(F32)
        return carry

    lax.fori_loop(1, 16, add_projected, 0)

    lane = lax.broadcasted_iota(jnp.int32, (64, 128), 1)
    low = lax.rem(lane, HDIM) < HDIM // 2
    row_id = lax.broadcasted_iota(jnp.int32, (128, 128), 0)
    col_id = lax.broadcasted_iota(jnp.int32, (128, 128), 1)
    same_head = jnp.where(row_id // HDIM == col_id // HDIM, 1.0, 0.0).astype(B16)

    def rotated(u):
        partner = jnp.where(low, pltpu.roll(u, 96, 1), pltpu.roll(u, 32, 1))
        return u * cosine[...] + partner * sine[...]

    query, keyed, valued, gated = [
        qkvg[:, 128 * i : 128 * (i + 1)].astype(B16).astype(F32) for i in range(4)
    ]
    q_rot = rotated(query).astype(B16).astype(F32)
    k_rot = (rotated(keyed) * 0.125).astype(B16).astype(F32)
    own = split_dot(q_rot * k_rot, same_head, 2).astype(B16).astype(F32)
    mixed[...] = q_rot
    retained[...] = own * valued
    for copy in here[7:]:
        copy.wait()
    pick_lane = lax.broadcasted_iota(jnp.int32, (HDIM, 128), 1)
    pick_row = lax.broadcasted_iota(jnp.int32, (HDIM, 128), 0)
    pick = jnp.where(lax.rem(pick_lane, HDIM) == pick_row, 1.0, 0.0)

    def attend(i, carry):
        rows = pl.ds(pl.multiple_of(i * 8, 8), 8)
        q = mixed[rows, :]
        products = (keys[rows].astype(F32) * q[:, None, :]).reshape(8 * BLK, 128)
        scores = split_dot(products, same_head, 2).reshape(8, BLK, 128)
        weights = (scores * factor[rows]).astype(B16).astype(F32)
        inner = jnp.sum(weights * values[rows].astype(F32), axis=1)
        spread = (q[:, None, :] * pick[None]).reshape(8 * HDIM, 128).astype(B16)
        wide = dot(spread, same_head).reshape(8, HDIM, 128)
        cross = jnp.sum(wide * state[rows], axis=1)
        carried = jnp.exp(-rate[...] * (offset[rows, :] + 1.0))
        retained[rows, :] += inner + cross * carried
        return carry

    lax.fori_loop(0, 8, attend, 0)
    kept = retained[...]
    centred = kept - split_dot(kept, same_head, 3) * (1.0 / HDIM)
    variance = split_dot(centred * centred, same_head, 3) * (1.0 / HDIM)
    normed = centred * lax.rsqrt(variance + EPS) * head_gain[...]
    heads = (gated / (1.0 + jnp.exp(-gated)) * normed).astype(B16)

    for used, copy in b_sends:

        @pl.when(used)
        def _():
            copy.wait_send()

    half = kv // 2
    m_out = d_out.at[0, :, pl.ds(0, 128)]
    d_out[0, :, 0:128] = heads

    @pl.when(owner)
    def _():
        m_all[half, c] = heads

    m_sends = []
    for k in range(16):
        dy, dx = k // 4, k % 4
        to = lax.rem(y + dy, 4), lax.rem(x + dx, 4)
        copy = copy_to(m_out, m_all.at[half, c], send.at[k], r_c.at[half, c], (*to, z, row_of))
        if k:
            copy.start()
        else:

            @pl.when(jnp.logical_not(owner))
            def _():
                copy.start()

        m_sends.append(copy)
    arrived(theirs[4], r_w.at[4])
    here[4].wait()

    for k, copy in enumerate(m_sends):
        if k:
            copy.wait_send()
        else:

            @pl.when(jnp.logical_not(owner))
            def _():
                copy.wait_send()

    d_sends = []
    for d in (4, 3, 5, 2, 6, 1, 7, 0):
        i = lax.rem(z + d, 8)
        for core in range(2):
            @pl.when(jnp.logical_not(jnp.logical_and(2 * i + c == kv, c == core)))
            def _():
                arrived(m_all.at[i, core], r_c.at[i, core])
        part = dot(m_all[i, 0], wo[0]) + dot(m_all[i, 1], wo[1])
        if d:
            d_out[i] = part.astype(B16)
            copy = copy_to(d_out.at[i], d_in.at[z], send.at[d], r_d.at[z], (y, x, i, c))
            copy.start()
            d_sends.append(copy)
        else:
            branch = part
    for d in NEAR[1:]:
        i = lax.rem(z + 8 - d, 8)
        arrived(d_in.at[i], r_d.at[i])
        branch = branch + d_in[i].astype(F32)
    for copy in d_sends:
        copy.wait_send()

    ones = jnp.full((8, 256), 1.0, B16)
    first = jnp.where(lax.broadcasted_iota(jnp.int32, (8, 256), 0) == 0, 1.0, 0.0).astype(B16)

    def row_sums(u):
        total = None
        for _ in range(3):
            part = u.astype(B16)
            u = u - part.astype(F32)
            term = lax.dot_general(ones, part, (((1,), (1,)), ((), ())), preferred_element_type=F32)
            total = term if total is None else total + term
        return total

    def column(u):
        total = None
        for _ in range(3):
            part = u.astype(B16)
            u = u - part.astype(F32)
            term = lax.dot_general(part, first, (((0,), (0,)), ((), ())), preferred_element_type=F32)
            total = term if total is None else total + term
        return total

    def normalized(values, gain, sums, sums_in, sem):
        sums[0] = row_sums(values)
        sums[1] = row_sums(values * values)
        sums_in[kv] = sums[...]
        copies = []
        for k in range(1, 16):
            to = (lax.rem(y + k // 4, 4), lax.rem(x + k % 4, 4), z, c)
            copies.append(copy_to(sums, sums_in.at[kv], send.at[k], sem.at[kv], to))
            copies[-1].start()
        for k in range(1, 16):
            i = lax.rem(y + k // 4, 4) * 4 + lax.rem(x + k % 4, 4)
            arrived(sums_in.at[i], sem.at[i])
        total = jnp.sum(sums_in[:, 0], axis=0) * (1.0 / 4096)
        square = jnp.sum(sums_in[:, 1], axis=0) * (1.0 / 4096)
        for copy in copies:
            copy.wait_send()
        scale = lax.rsqrt(square - total * total + EPS)
        return (values - column(total)) * column(scale) * gain[...]

    tall = ALPHA * tok[...].astype(F32) + branch
    rows_now = normalized(tall, mixer_gain, s_out, s_in, r_e).astype(B16)
    hidden[...] = rows_now
    h_all[z] = rows_now

    h_sends = []
    for d in NEAR[1:]:
        h_sends.append(copy_to(hidden, h_all.at[z], send.at[d], r_f.at[z], (y, x, lax.rem(z + d, 8), c)))
        h_sends[-1].start()
    for i in (5, 6):
        here[i].wait()
        arrived(theirs[i], r_w.at[i])

    def up_block(d, carry):
        zp = lax.rem(z + 8 - d, 8)

        @pl.when(d > 0)
        def _():
            arrived(h_all.at[zp], r_f.at[zp])

        yd = zp // 2
        xd = lax.rem(zp, 2) * 2
        rows = h_all[zp]
        first_half = dot(rows, wu[0]).astype(B16)
        second_half = dot(rows, wu[1]).astype(B16)
        for side in range(2):
            to_x = xd + side
            g1_out[0, to_x, yd] = first_half[32 * side : 32 * side + 32]
            g1_out[1, yd, to_x] = second_half[32 * side : 32 * side + 32]

        return carry

    for d in NEAR:
        up_block(d, 0)
    for copy in h_sends:
        copy.wait_send()

    along = (x, y)

    def device_on(colour, stage, index):
        if (colour + stage) % 2 == 0:
            return (y, index, z, c)
        return (index, x, z, c)

    g1_sends = []
    for j in (1, 3, 2, 0):
        for d in (2, 1, 3):
            for colour in range(2):
                me, other = along[colour], along[1 - colour]
                to, piece = lax.rem(me + d, 4), lax.rem(other + j, 4)
                copy = copy_to(
                    g1_out.at[colour, to, piece], g1_in.at[colour, me, piece],
                    send.at[len(g1_sends)], r_g1.at[colour, me, piece], device_on(colour, 0, to),
                )
                copy.start()
                g1_sends.append(copy)
    g2_sends = []
    for j in (1, 3, 2, 0):
        for colour in range(2):
            me, other = along[colour], along[1 - colour]
            piece = lax.rem(other + j, 4)
            total = g1_out[colour, me, piece].astype(F32)
            for d in (1, 3, 2):
                source = lax.rem(me + d, 4)
                arrived(g1_in.at[colour, source, piece], r_g1.at[colour, source, piece])
                total = total + g1_in[colour, source, piece].astype(F32)
            if j:
                g2_out[colour, piece] = total.astype(B16)
                copy = copy_to(
                    g2_out.at[colour, piece], g2_in.at[colour, other],
                    send.at[24 + len(g2_sends)], r_g2.at[colour, other], device_on(colour, 1, piece),
                )
                copy.start()
                g2_sends.append(copy)
            else:
                f_out[colour] = total
    for copy in g1_sends:
        copy.wait_send()

    def place(colour, i, j):
        if colour == 0:
            return (colour, i, j)
        return (colour, j, i)

    h1_sends = []
    h2_sends = []
    for colour in range(2):
        me, other = along[colour], along[1 - colour]
        total = f_out[colour]
        for d in (1, 3, 2):
            source = lax.rem(other + d, 4)
            arrived(g2_in.at[colour, source], r_g2.at[colour, source])
            total = total + g2_in[colour, source].astype(F32)
        active = jnp.square(jnp.maximum(total, 0.0)).astype(B16)
        spot = act_all.at[colour, y, x]
        act_all[colour, y, x] = active
        for d in (2, 1, 3):
            to = lax.rem(other + d, 4)
            copy = copy_to(
                spot, spot, send.at[len(h1_sends)], r_h1.at[colour, other], device_on(colour, 1, to)
            )
            copy.start()
            h1_sends.append(copy)
        for d in (2, 1, 3):
            to = lax.rem(me + d, 4)
            copy = copy_to(
                spot, spot, send.at[6 + len(h2_sends)], r_h2.at[colour, other, me], device_on(colour, 0, to)
            )
            copy.start()
            h2_sends.append(copy)
    for copy in g2_sends:
        copy.wait_send()
    for j in (1, 3, 2):
        for colour in range(2):
            me, other = along[colour], along[1 - colour]
            source = lax.rem(other + j, 4)
            spot = act_all.at[place(colour, source, me)]
            arrived(spot, r_h1.at[colour, source])
            for d in (2, 1, 3):
                to = lax.rem(me + d, 4)
                copy = copy_to(
                    spot, spot, send.at[6 + len(h2_sends)], r_h2.at[colour, source, me],
                    device_on(colour, 0, to),
                )
                copy.start()
                h2_sends.append(copy)
    for j in (0, 1, 3, 2):
        for d in (1, 3, 2):
            for colour in range(2):
                me, other = along[colour], along[1 - colour]
                source, at = lax.rem(other + j, 4), lax.rem(me + d, 4)
                arrived(act_all.at[place(colour, source, at)], r_h2.at[colour, source, at])
    for copy in h1_sends + h2_sends:
        copy.wait_send()

    e_sends = []
    for d in (4, 3, 5, 2, 6, 1, 7, 0):
        i = lax.rem(z + d, 8)
        yd, xd = i // 2, lax.rem(i, 2) * 2
        part = None
        for colour in range(2):
            rows = act_all[colour, yd, pl.ds(xd, 2)].reshape(64, 1024)
            term = dot(rows, wd[colour])
            part = term if part is None else part + term
        if d:
            e_out[i] = part.astype(B16)
            copy = copy_to(e_out.at[i], e_in.at[z], send.at[d], r_i.at[z], (y, x, i, c))
            copy.start()
            e_sends.append(copy)
        else:
            downward = part
    for d in NEAR[1:]:
        i = lax.rem(z + 8 - d, 8)
        arrived(e_in.at[i], r_i.at[i])
        downward = downward + e_in[i].astype(F32)
    for copy in e_sends:
        copy.wait_send()
    tall = ALPHA * hidden[...].astype(F32) + downward
    out[...] = normalized(tall, final_gain, s_out, f_in, r_j).astype(B16)


def per_device(
    tokens, lengths, state_block, cached_keys, cached_values, query_weight, key_weight,
    value_weight, gate_weight, decay_rate, head_gain, out_weight, mixer_gain, up_weight,
    down_weight, final_gain,
):
    half = HDIM // 2
    inverse = 10000.0 ** (-jnp.arange(half, dtype=F32) / half)
    angle = lengths.astype(F32)[:, None] * inverse[None, :]
    cosine, sine = jnp.cos(angle), jnp.sin(angle)
    cosine = jnp.concatenate([cosine] * 4, 1)
    sine = jnp.concatenate([-sine, sine] * 2, 1)
    offset = jnp.broadcast_to((lengths % BLK).astype(F32)[:, None], (64, 128))
    rate = jnp.repeat(decay_rate, HDIM)[None, :]
    vmem = pl.BlockSpec(memory_space=pltpu.VMEM)
    anywhere = pl.BlockSpec(memory_space=pl.ANY)
    dma = pltpu.SemaphoreType.DMA
    scratch = [
        pltpu.VMEM((64, 64, 128), F32),
        pltpu.VMEM((64, 128, 128), B16),
        pltpu.VMEM((64, 128, 128), B16),
        pltpu.VMEM((64, 128, 128), F32),
        pltpu.VMEM((2, 256, 512), B16),
        pltpu.VMEM((2, 128, 256), B16),
        pltpu.VMEM((2, 256, 1024), B16),
        pltpu.VMEM((2, 1024, 256), B16),
        pltpu.VMEM((8, 64, 256), B16),
        pltpu.VMEM((8, 2, 64, 512), B16),
        pltpu.VMEM((16, 64, 512), B16),
        pltpu.VMEM((64, 512), F32),
        pltpu.VMEM((64, 128), F32),
        pltpu.VMEM((64, 128), F32),
        pltpu.VMEM((8, 2, 64, 128), B16),
        pltpu.VMEM((8, 64, 256), B16),
        pltpu.VMEM((8, 64, 256), B16),
        pltpu.VMEM((2, 8, 64), F32),
        pltpu.VMEM((16, 2, 8, 64), F32),
        pltpu.VMEM((64, 256), B16),
        pltpu.VMEM((8, 64, 256), B16),
        pltpu.VMEM((2, 4, 4, 32, 1024), B16),
        pltpu.VMEM((2, 4, 4, 32, 1024), B16),
        pltpu.VMEM((2, 4, 32, 1024), B16),
        pltpu.VMEM((2, 4, 32, 1024), B16),
        pltpu.VMEM((2, 4, 4, 32, 1024), B16),
        pltpu.VMEM((8, 64, 256), B16),
        pltpu.VMEM((8, 64, 256), B16),
        pltpu.VMEM((2, 32, 1024), F32),
        pltpu.VMEM((16, 2, 8, 64), F32),
        dma((10,)),
        dma((40,)),
        dma((7,)),
        dma((8,)),
        dma((16,)),
        dma((8, 2)),
        dma((8,)),
        dma((16,)),
        dma((8,)),
        dma((2, 4, 4)),
        dma((2, 4)),
        dma((2, 4)),
        dma((2, 4, 4)),
        dma((8,)),
        dma((16,)),
    ]
    return pl.pallas_call(
        kernel,
        out_shape=jax.ShapeDtypeStruct((64, 256), B16),
        in_specs=[vmem] * 8 + [anywhere] * 10,
        out_specs=vmem,
        scratch_shapes=scratch,
        name="layer",
        compiler_params=pltpu.CompilerParams(
            collective_id=0, has_side_effects=True, vmem_limit_bytes=56 * 1024 * 1024
        ),
    )(
        tokens, cosine, sine, offset, rate, head_gain[None, :], mixer_gain[None, :], final_gain[None, :],
        state_block, cached_keys, cached_values, query_weight, key_weight, value_weight, gate_weight,
        out_weight, up_weight, down_weight,
    )


def solution(mesh):
    finer = Mesh(mesh.devices.reshape(4, 4, 8, 2), AXES)
    kv, tp = ("y", "x"), ("z", "c")
    placed = (
        P(tp, kv), P(kv), P(kv, None, tp), P(kv, None, tp), P(kv, None, tp),
        P(kv, tp), P(kv, tp), P(kv, tp), P(kv, tp), P(tp), P(tp), P(tp, kv), P(kv),
        P(kv, tp), P(tp, kv), P(kv),
    )
    return jax.shard_map(per_device, mesh=finer, in_specs=placed, out_specs=P(tp, kv), check_vma=False)
```

time: 298 us -> 114 us (0.38)
  blocking collectives: 242 us -> 0 us
  Pallas kernels: 0 us -> 109 us
  waiting for transfers between devices: 16 us -> 0 us
  local copies, waits for them, and re-layouts: 17.1 us -> 3.44 us
  matrix products: 7.98 us -> 0 us
  starting transfers between devices: 7.61 us -> 0 us
  other arithmetic: 5.97 us -> 1.69 us
    all_to_all x7 -> x0, blocking collectives: 207 us -> none  [the longest x3 114 us: sent_and_summed(): lax.all_to_all(parts, axis, split_axis=0, concat_axis=0, tiled=True)]
    pallas_call x0 -> x1, Pallas kernels: none -> 109 us  [per_device(): pl.pallas_call(kernel, out_shape=jax.ShapeDtypeStruct((64, 256), B16), in...]
    psum x4 -> x0, blocking collectives: 35.5 us -> none  [by_axis(): return functools.reduce(lax.psum, axes, x)]
    all_to_all x1 -> x0, waiting for transfers between devices: 16 us -> none  [sent_and_summed(): lax.all_to_all(parts, axis, split_axis=0, concat_axis=0, tiled=True)]
    dot_general x10 -> x0, matrix products: 7.98 us -> none  [the longest x1 2.38 us: retain(): jnp.einsum('shk,skhv->shv', q_rot.astype(jnp.float32), state.reshape(coun...]
    all_to_all x1 -> x0, starting transfers between devices: 7.61 us -> none  [sent_and_summed(): lax.all_to_all(parts, axis, split_axis=0, concat_axis=0, tiled=True)]
    unnamed x30 -> x1, local copies, waits for them, and re-layouts: 8.22 us -> 1.38 us
    reshape x5 -> x0, local copies, waits for them, and re-layouts: 5.52 us -> none  [the longest x1 5.14 us: retain(): state.reshape(count, HDIM, heads, HDIM)]
  transfers between devices with their start and end apart: 1 -> 0, of which waited for: 1 -> 0; matrix products, arithmetic and copies ran while one was open for 5% -> 0% of each run, Pallas kernels for 0% -> 0%
where the time goes in v2:
time: 114 us
  Pallas kernels  109 us (96%)
  local copies, waits for them, and re-layouts  3.44 us (3%)
  other arithmetic  1.69 us (1%)
    pallas_call x1, Pallas kernels, per_device(): pl.pallas_call(kernel, out_shape=jax.ShapeDtypeStruct((64, 256), B16), in...  109 us

profile of v2, /device:TPU:2, one launch (start us, length us, event | category | flops | bytes accessed | tf_op | source)
XLA Modules:
  0.0 114.0 jit_solution(775566075049232937)
XLA Ops:
  0.0 0.7 fusion.1
  0.8 0.2 fusion
  1.0 0.7 pad_maximum_fusion
  1.7 0.7 broadcast_in_dim.20.offset
  2.4 0.7 broadcast_in_dim.21
  3.1 0.7 broadcast_in_dim_reshape.3.rate
  3.8 108.9 %layer.1 = bf16[64,256]{1,0:T(8,128)(2,1)} custom-call(bf16[64,256]{1,0:T(8,128)(2,1)} %tok.1, f32[64,128]{1,0:T(8,128)} %get-tuple-element.10.cosine, f32[64,128]{1,0:T(8,128)} %get-tuple-element.11.sine, f32[64,128]{1,0:T(8,128)} %broadcast_in_dim.20.offset, f32[1,128]{1,0:T(1,128)} %broadcast_in_dim_reshape.3.rate, f32[1,128]{1,0:T(1,128)} %bitcast.5, ...), custom_call_target="tpu_custom_call" | custom-call | tf_op jit(solution)/shard_map/layer/pallas_call | solution.py:537
  112.6 1.4 %copy.18 = bf16[64,256]{1,0:T(8,128)(2,1)} copy(bf16[64,256]{1,0:T(8,128)(2,1)} %layer.1) | data formatting | bytes 65536
  (1 shorter events, 0.0 us)

commit v3 on v2

v3 whole, which is shorter than its diff:
```python
import functools

import jax
import jax.numpy as jnp
from jax import lax
from jax.experimental import pallas as pl
from jax.experimental.pallas import tpu as pltpu
from jax.sharding import Mesh
from jax.sharding import PartitionSpec as P

HDIM = 64
BLK = 128
ALPHA = 2.0**0.5
EPS = 1e-05
AXES = ("y", "x", "z", "c")
NEAR = (0, 1, 7, 2, 6, 3, 5, 4)
F32 = jnp.float32
B16 = jnp.bfloat16


def dot(a, b):
    return jnp.dot(a, b, preferred_element_type=F32)


def split_dot(a, b, terms, left=True):
    total = None
    rest = a if left else b
    for _ in range(terms):
        part = rest.astype(B16)
        rest = rest - part.astype(F32)
        term = dot(part, b) if left else dot(a, part)
        total = term if total is None else total + term
    return total


def copy_to(src, dst, send, recv, device):
    return pltpu.make_async_remote_copy(
        src_ref=src,
        dst_ref=dst,
        send_sem=send,
        recv_sem=recv,
        device_id=device,
        device_id_type=pl.DeviceIdType.MESH,
    )


def kernel(
    tok, lengths, head_gain, mixer_gain, final_gain, rates,
    state_h, keys_h, values_h, wq_h, wk_h, wv_h, wg_h, wo_h, wu_h, wd_h,
    out,
    state, keys, values, factor, wp, wo, wu, wd, cosine, sine, offset,
    t_all, b1_out, b1_in0, b1_in1, b2_out, b2_in, retained, turned, heads, m_all, d_out, d_in,
    s_out, s_in, p_out, p_in, col_out, col_in, ends, lift, payload, hidden, h_all,
    g1_out, g1_in, g2_out, g2_in, g_sum, act_all, e_sum, e_out, e_in, j_out, j_in,
    local, send, r_w, r_a, r_b10, r_b11, r_b2, r_c, r_d, r_e, r_p, r_col, r_f, r_g1, r_g2, r_h1, r_h2, r_i, r_j,
):
    y, x, z, c = [lax.axis_index(name) for name in AXES]
    kv = y * 4 + x
    sibling = (y, x, z, 1 - c)
    row_of = lax.rem(x, 2)
    owner = row_of == c
    used = [0]
    pending = []

    def put(src, dst, recv, device, when=None):
        copy = copy_to(src, dst, send.at[used[0]], recv, device)
        used[0] += 1
        if when is None:
            copy.start()
        else:

            @pl.when(when)
            def _():
                copy.start()

        pending.append((when, copy))

    def settle():
        for when, copy in pending:
            if when is None:
                copy.wait_send()
            else:

                @pl.when(when)
                def _():
                    copy.wait_send()

        pending.clear()
        used[0] = 0

    def arrived(dst, sem, when=None):
        copy = copy_to(dst, dst, send.at[0], sem, sibling)
        if when is None:
            copy.wait_recv()
        else:

            @pl.when(when)
            def _():
                copy.wait_recv()

    here = []

    def fetch(src, dst):
        here.append(pltpu.make_async_copy(src, dst, local.at[len(here)]))
        here[-1].start()

    quarter = [wp.at[c, :, pl.ds(128 * i, 128)] for i in range(4)]
    for src, dst in zip((wq_h, wk_h, wv_h, wg_h), quarter):
        fetch(src, dst)
    fetch(wo_h, wo.at[c])
    fetch(wu_h, wu.at[c])
    fetch(wd_h, wd.at[c])
    fetch(keys_h, keys)
    fetch(values_h, values)
    fetch(state_h, state)

    barrier = pltpu.get_barrier_semaphore()
    greeted = 0
    for dy in range(4):
        for dx in range(4):
            for dc in range(2):
                if dy or dx or dc:
                    peer = (lax.rem(y + dy, 4), lax.rem(x + dx, 4), z, lax.rem(c + dc, 2))
                    pl.semaphore_signal(barrier, inc=1, device_id=peer, device_id_type=pl.DeviceIdType.MESH)
                    greeted += 1
    for dz in range(1, 8):
        peer = (y, x, lax.rem(z + dz, 8), c)
        pl.semaphore_signal(barrier, inc=1, device_id=peer, device_id_type=pl.DeviceIdType.MESH)
        greeted += 1

    ones = jnp.full((8, 256), 1.0, B16)
    first = jnp.where(lax.broadcasted_iota(jnp.int32, (8, 256), 0) == 0, 1.0, 0.0).astype(B16)
    lane = lax.broadcasted_iota(jnp.int32, (64, 128), 1)
    low = lax.rem(lane, HDIM) < HDIM // 2
    lane_row = lax.broadcasted_iota(jnp.int32, (1, 128), 1)
    rate = jnp.where(lane_row < HDIM, rates[0], rates[1])

    def row_sums(u):
        total = None
        for _ in range(3):
            part = u.astype(B16)
            u = u - part.astype(F32)
            term = lax.dot_general(ones, part, (((1,), (1,)), ((), ())), preferred_element_type=F32)
            total = term if total is None else total + term
        return total

    def column(u):
        total = None
        for _ in range(3):
            part = u.astype(B16)
            u = u - part.astype(F32)
            term = lax.dot_general(part, first, (((0,), (0,)), ((), ())), preferred_element_type=F32)
            total = term if total is None else total + term
        return total

    position = column(jnp.broadcast_to(lengths[...].astype(F32), (8, 64)))[:, :128]
    offset[...] = position - jnp.floor(position * (1.0 / BLK)) * BLK
    inverse = jnp.zeros((1, 128), F32)
    for i in range(HDIM // 2):
        inverse = jnp.where(lax.rem(lane_row, HDIM // 2) == i, 10000.0 ** (-i / (HDIM // 2)), inverse)
    angle = position * inverse
    cosine[...] = jnp.cos(angle)
    sines = jnp.sin(angle)
    sine[...] = jnp.where(low, -sines, sines)

    def decay(i, carry):
        rows = pl.ds(pl.multiple_of(i * 8, 8), 8)
        off = offset[rows, :][:, None, :]
        slot = lax.broadcasted_iota(jnp.int32, (8, BLK, 128), 1).astype(F32)
        lag = jnp.maximum(off - slot, 0.0)
        factor[rows] = jnp.where(slot < off, jnp.exp(-rate[None] * lag), 0.0)
        return carry

    lax.fori_loop(0, 8, decay, 0)
    t_all[z] = tok[...]
    pl.semaphore_wait(barrier, greeted)

    for d in NEAR[1:]:
        put(tok, t_all.at[z], r_a.at[z], (y, x, lax.rem(z + d, 8), c))
    for i, (src, dst) in enumerate(
        [*zip((wq_h, wk_h, wv_h, wg_h), quarter), (wo_h, wo.at[c]), (wu_h, wu.at[c]), (wd_h, wd.at[c])]
    ):
        put(src, dst, r_w.at[i], sibling)
    theirs = [wp.at[1 - c, :, pl.ds(128 * i, 128)] for i in range(4)] + [w.at[1 - c] for w in (wo, wu, wd)]
    for i in range(4):
        here[i].wait()
        arrived(theirs[i], r_w.at[i])

    for d in NEAR:
        zp = lax.rem(z + 8 - d, 8)
        if d:
            arrived(t_all.at[zp], r_a.at[zp])
        yd, side = zp // 2, lax.rem(zp, 2)
        xd = 2 * side + c
        rows = t_all[zp]
        for colour in range(2):
            part = dot(rows, wp[colour]).astype(B16)
            b1_out[zp, colour] = part
            if colour == 0:
                mine, dst, sem, to = xd == x, b1_in0.at[x, yd], r_b10.at[x, yd], (y, xd, z, c)
            else:
                mine, dst, sem, to = yd == y, b1_in1.at[y, side], r_b11.at[y, side], (yd, x, z, c)

            @pl.when(mine)
            def _():
                dst[...] = part

            put(b1_out.at[zp, colour], dst, sem, to, jnp.logical_not(mine))

    def first_stage_x(j):
        piece = lax.rem(z // 2 + j, 4)

        @pl.when(owner)
        def _():
            for k in (1, 3, 2):
                i = lax.rem(x + k, 4)
                arrived(b1_in0.at[i, piece], r_b10.at[i, piece])
            total = b1_in0[0, piece].astype(F32)
            for k in range(1, 4):
                total = total + b1_in0[k, piece].astype(F32)
            b2_out[j] = total.astype(B16)

        mine = jnp.logical_and(piece == y, c == 0)

        @pl.when(jnp.logical_and(owner, mine))
        def _():
            b2_in[y] = b2_out[j]

        put(
            b2_out.at[j], b2_in.at[y], r_b2.at[y], (piece, x, z, 0),
            jnp.logical_and(owner, jnp.logical_not(mine)),
        )

    def first_stage_y(j):
        side = lax.rem(z + j, 2)
        for k in (1, 3, 2):
            i = lax.rem(y + k, 4)
            arrived(b1_in1.at[i, side], r_b11.at[i, side])
        total = b1_in1[0, side].astype(F32)
        for k in range(1, 4):
            total = total + b1_in1[k, side].astype(F32)
        total = total.astype(B16)
        b2_out[4 + j] = total
        xd = 2 * side + c
        mine = jnp.logical_and(xd == x, c == 1)

        @pl.when(mine)
        def _():
            b2_in[x] = total

        put(b2_out.at[4 + j], b2_in.at[x], r_b2.at[x], (y, xd, z, 1), jnp.logical_not(mine))

    first_stage_x(0)
    first_stage_x(1)
    first_stage_y(0)
    first_stage_x(3)
    first_stage_y(1)
    first_stage_x(2)

    for i in (5, 6):
        here[i].wait()
        arrived(theirs[i], r_w.at[i])
    gain_rows = jnp.broadcast_to(mixer_gain[...], (8, 256))
    for half in range(2):
        col_out[:, pl.ds(1024 * half, 1024)] = split_dot(gain_rows, wu[half], 3)[0:1]
    col_in[kv] = col_out[...]
    for k in (5, 7, 13, 15, 6, 14, 9, 11, 10, 1, 4, 3, 12, 2, 8):
        to = (lax.rem(y + k // 4, 4), lax.rem(x + k % 4, 4), z, c)
        put(col_out, col_in.at[kv], r_col.at[kv], to)

    place_b2 = jnp.where(c == 0, y, x)
    for k in range(4):
        arrived(b2_in.at[k], r_b2.at[k], jnp.logical_not(jnp.logical_and(owner, place_b2 == k)))
    qkvg = b2_in[0].astype(F32)
    for k in range(1, 4):
        qkvg = qkvg + b2_in[k].astype(F32)

    row_id = lax.broadcasted_iota(jnp.int32, (128, 128), 0)
    col_id = lax.broadcasted_iota(jnp.int32, (128, 128), 1)
    same_head = jnp.where(row_id // HDIM == col_id // HDIM, 1.0, 0.0).astype(B16)

    def rotated(u):
        partner = jnp.where(low, pltpu.roll(u, 96, 1), pltpu.roll(u, 32, 1))
        return u * cosine[...] + partner * sine[...]

    query, keyed, valued, gated = [
        qkvg[:, 128 * i : 128 * (i + 1)].astype(B16).astype(F32) for i in range(4)
    ]
    q_rot = rotated(query).astype(B16).astype(F32)
    k_rot = (rotated(keyed) * 0.125).astype(B16).astype(F32)
    own = split_dot(q_rot * k_rot, same_head, 2).astype(B16).astype(F32)
    turned[...] = q_rot
    retained[...] = own * valued
    for copy in here[7:]:
        copy.wait()
    pick_lane = lax.broadcasted_iota(jnp.int32, (HDIM, 128), 1)
    pick_row = lax.broadcasted_iota(jnp.int32, (HDIM, 128), 0)
    pick = jnp.where(lax.rem(pick_lane, HDIM) == pick_row, 1.0, 0.0)

    def attend(i, carry):
        rows = pl.ds(pl.multiple_of(i * 8, 8), 8)
        q = turned[rows, :]
        products = (keys[rows].astype(F32) * q[:, None, :]).reshape(8 * BLK, 128)
        scores = split_dot(products, same_head, 2).reshape(8, BLK, 128)
        weights = (scores * factor[rows]).astype(B16).astype(F32)
        inner = jnp.sum(weights * values[rows].astype(F32), axis=1)
        spread = (q[:, None, :] * pick[None]).reshape(8 * HDIM, 128).astype(B16)
        wide = dot(spread, same_head).reshape(8, HDIM, 128)
        cross = jnp.sum(wide * state[rows], axis=1)
        carried = jnp.exp(-rate * (offset[rows, :] + 1.0))
        retained[rows, :] += inner + cross * carried
        return carry

    lax.fori_loop(0, 8, attend, 0)
    kept = retained[...]
    centred = kept - split_dot(kept, same_head, 3) * (1.0 / HDIM)
    variance = split_dot(centred * centred, same_head, 3) * (1.0 / HDIM)
    normed = centred * lax.rsqrt(variance + EPS) * head_gain[...]
    mixed = (gated / (1.0 + jnp.exp(-gated)) * normed).astype(B16)
    heads[...] = mixed
    half = kv // 2

    for k in (10, 5, 7, 13, 15, 6, 14, 9, 11, 1, 4, 3, 12, 2, 8, 0):
        to = (lax.rem(y + k // 4, 4), lax.rem(x + k % 4, 4), z, row_of)
        put(heads, m_all.at[half, c], r_c.at[half, c], to, None if k else jnp.logical_not(owner))

    @pl.when(owner)
    def _():
        m_all[half, c] = mixed

    here[4].wait()
    arrived(theirs[4], r_w.at[4])

    start = 2 * y + x // 2
    for j in (0, 1, 7, 2, 6, 3, 5, 4):
        i = lax.rem(start + j, 8)
        for core in range(2):
            arrived(
                m_all.at[i, core], r_c.at[i, core],
                jnp.logical_not(jnp.logical_and(2 * i + c == kv, c == core)),
            )
        part = (dot(m_all[i, 0], wo[0]) + dot(m_all[i, 1], wo[1])).astype(B16)
        mine = i == z

        @pl.when(mine)
        def _():
            d_in[i] = part

        d_out[i] = part
        put(d_out.at[i], d_in.at[z], r_d.at[z], (y, x, i, c), jnp.logical_not(mine))
    branch = d_in[z].astype(F32)
    for d in NEAR[1:]:
        i = lax.rem(z + 8 - d, 8)
        arrived(d_in.at[i], r_d.at[i])
        branch = branch + d_in[i].astype(F32)

    tall = ALPHA * tok[...].astype(F32) + branch
    part_mean = jnp.sum(tall, axis=1, keepdims=True) * (1.0 / 256)
    part_centred = tall - part_mean
    scaled = (part_centred * mixer_gain[...]).astype(B16)
    payload[...] = scaled
    h_all[z] = scaled
    for d in (4, 3, 5, 2, 6, 1, 7):
        put(payload, h_all.at[z], r_f.at[z], (y, x, lax.rem(z + d, 8), c))
    s_out[0] = row_sums(jnp.broadcast_to(part_mean, (64, 256))) * (1.0 / 256)
    s_out[1] = row_sums(part_centred * part_centred)
    s_in[kv] = s_out[...]
    for k in (10, 5, 7, 13, 15, 6, 14, 9, 11, 1, 4, 3, 12, 2, 8):
        to = (lax.rem(y + k // 4, 4), lax.rem(x + k % 4, 4), z, c)
        put(s_out, s_in.at[kv], r_e.at[kv], to)

    along = (x, y)

    def device_on(colour, stage, index):
        if (colour + stage) % 2 == 0:
            return (y, index, z, c)
        return (index, x, z, c)

    for d in NEAR:
        zp = lax.rem(z + 8 - d, 8)
        if d:
            arrived(h_all.at[zp], r_f.at[zp])
        yd, xd = zp // 2, lax.rem(zp, 2) * 2
        rows = h_all[zp]
        for colour in range(2):
            part = dot(rows, wu[colour]).astype(B16)
            for side in range(2):
                rows_of = part[32 * side : 32 * side + 32]
                me, to, piece = (x, xd + side, yd) if colour == 0 else (y, yd, xd + side)
                g1_out[colour, to, piece] = rows_of
                put(
                    g1_out.at[colour, to, piece], g1_in.at[colour, me, piece],
                    r_g1.at[colour, me, piece], device_on(colour, 0, to), to != me,
                )

    for k in (1, 4, 3, 12, 2, 8, 5, 7, 13, 15, 6, 14, 9, 11, 10):
        i = lax.rem(y + k // 4, 4) * 4 + lax.rem(x + k % 4, 4)
        arrived(s_in.at[i], r_e.at[i])
    means = s_in[:, 0]
    mean = jnp.sum(means, axis=0) * (1.0 / 16)
    shift = means - mean[None]
    spread = (jnp.sum(s_in[:, 1], axis=0) + 256.0 * jnp.sum(shift * shift, axis=0)) * (1.0 / 4096)
    scale = lax.rsqrt(spread + EPS)
    eight = lax.broadcasted_iota(jnp.int32, (8, 64), 0)
    for group in range(2):
        stacked = jnp.zeros((8, 64), F32)
        for k in range(8):
            stacked = jnp.where(eight == k, shift[8 * group + k], stacked)
        p_out[group] = stacked
    p_out[2] = scale
    mine = half == z

    @pl.when(mine)
    def _():
        p_in[...] = p_out[...]

    for d in range(1, 8):
        put(p_out, p_in, r_p.at[0], (y, x, lax.rem(z + d, 8), c), mine)
    own_shift = s_out[0] - mean
    hidden[...] = ((part_centred + column(own_shift)) * column(scale) * mixer_gain[...]).astype(B16)

    for k in range(1, 16):
        i = lax.rem(y + k // 4, 4) * 4 + lax.rem(x + k % 4, 4)
        arrived(col_in.at[i], r_col.at[i])
    wide_eight = lax.broadcasted_iota(jnp.int32, (8, 2048), 0)
    arrived(p_in, r_p.at[0], jnp.logical_not(mine))
    lifted = jnp.zeros((64, 2048), F32)
    for group in range(2):
        stacked = jnp.zeros((8, 2048), F32)
        for k in range(8):
            stacked = jnp.where(wide_eight == k, col_in[8 * group + k], stacked)
        shift_high = p_in[group].astype(B16)
        shift_low = (p_in[group] - shift_high.astype(F32)).astype(B16)
        col_high = stacked.astype(B16)
        col_low = (stacked - col_high.astype(F32)).astype(B16)
        for a, b in ((shift_high, col_high), (shift_high, col_low), (shift_low, col_high)):
            lifted = lifted + lax.dot_general(a, b, (((0,), (0,)), ((), ())), preferred_element_type=F32)
    upper = row_of == 1
    lift[...] = jnp.where(upper, lifted[32:], lifted[:32])
    scales = column(p_in[2])
    ends[...] = jnp.where(upper, scales[32:], scales[:32])

    for j in (0, 1, 3, 2):
        for colour in range(2):
            me, other = along[colour], along[1 - colour]
            piece = lax.rem(other + j, 4)
            total = g1_out[colour, me, piece].astype(F32)
            for d in (1, 3, 2):
                source = lax.rem(me + d, 4)
                arrived(g1_in.at[colour, source, piece], r_g1.at[colour, source, piece])
                total = total + g1_in[colour, source, piece].astype(F32)
            if j:
                g2_out[colour, piece] = total.astype(B16)
                put(
                    g2_out.at[colour, piece], g2_in.at[colour, other], r_g2.at[colour, other],
                    device_on(colour, 1, piece),
                )
            else:
                g_sum[colour] = total + lift[:, 1024 * colour : 1024 * colour + 1024]

    def place(colour, i, j):
        if colour == 0:
            return (colour, i, j)
        return (colour, j, i)

    for colour in range(2):
        me, other = along[colour], along[1 - colour]
        total = g_sum[colour]
        for d in (1, 3, 2):
            source = lax.rem(other + d, 4)
            arrived(g2_in.at[colour, source], r_g2.at[colour, source])
            total = total + g2_in[colour, source].astype(F32)
        times = jnp.concatenate([ends[...]] * 4, 1)
        active = jnp.square(jnp.maximum(total * times, 0.0)).astype(B16)
        spot = act_all.at[colour, y, x]
        act_all[colour, y, x] = active
        for d in (2, 1, 3):
            put(spot, spot, r_h1.at[colour, other], device_on(colour, 1, lax.rem(other + d, 4)))
        for d in (2, 1, 3):
            put(spot, spot, r_h2.at[colour, other, me], device_on(colour, 0, lax.rem(me + d, 4)))
    for j in (1, 3, 2):
        for colour in range(2):
            me, other = along[colour], along[1 - colour]
            source = lax.rem(other + j, 4)
            spot = act_all.at[place(colour, source, me)]
            arrived(spot, r_h1.at[colour, source])
            for d in (2, 1, 3):
                put(spot, spot, r_h2.at[colour, source, me], device_on(colour, 0, lax.rem(me + d, 4)))

    for j in (0, 1, 3, 2):
        for colour in range(2):
            me, other = along[colour], along[1 - colour]
            source = lax.rem(other + j, 4)
            for d in (1, 3, 2):
                at = lax.rem(me + d, 4)
                arrived(act_all.at[place(colour, source, at)], r_h2.at[colour, source, at])
            if colour == 0:
                rows = act_all[0, source].reshape(128, 1024)
            else:
                rows = act_all[1, :, source].reshape(128, 1024)
            e_sum[colour, source] = dot(rows, wd[colour]).reshape(4, 32, 256)
    for d in (4, 3, 5, 2, 6, 1, 7, 0):
        i = lax.rem(z + d, 8)
        yd, xd = i // 2, lax.rem(i, 2) * 2
        part = jnp.concatenate(
            [e_sum[0, yd, xd + side] + e_sum[1, xd + side, yd] for side in range(2)], 0
        )
        if d:
            e_out[i] = part.astype(B16)
            put(e_out.at[i], e_in.at[z], r_i.at[z], (y, x, i, c))
        else:
            downward = part
    for d in NEAR[1:]:
        i = lax.rem(z + 8 - d, 8)
        arrived(e_in.at[i], r_i.at[i])
        downward = downward + e_in[i].astype(F32)

    tall = ALPHA * hidden[...].astype(F32) + downward
    part_mean = jnp.sum(tall, axis=1, keepdims=True) * (1.0 / 256)
    part_centred = tall - part_mean
    j_out[0] = row_sums(jnp.broadcast_to(part_mean, (64, 256))) * (1.0 / 256)
    j_out[1] = row_sums(part_centred * part_centred)
    j_in[kv] = j_out[...]
    for k in (10, 5, 7, 13, 15, 6, 14, 9, 11, 1, 4, 3, 12, 2, 8):
        to = (lax.rem(y + k // 4, 4), lax.rem(x + k % 4, 4), z, c)
        put(j_out, j_in.at[kv], r_j.at[kv], to)
    for k in range(1, 16):
        i = lax.rem(y + k // 4, 4) * 4 + lax.rem(x + k % 4, 4)
        arrived(j_in.at[i], r_j.at[i])
    means = j_in[:, 0]
    mean = jnp.sum(means, axis=0) * (1.0 / 16)
    shift = means - mean[None]
    spread = (jnp.sum(j_in[:, 1], axis=0) + 256.0 * jnp.sum(shift * shift, axis=0)) * (1.0 / 4096)
    scale = lax.rsqrt(spread + EPS)
    out[...] = ((part_centred + column(j_out[0] - mean)) * column(scale) * final_gain[...]).astype(B16)
    settle()


def per_device(
    tokens, lengths, state_block, cached_keys, cached_values, query_weight, key_weight,
    value_weight, gate_weight, decay_rate, head_gain, out_weight, mixer_gain, up_weight,
    down_weight, final_gain,
):
    vmem = pl.BlockSpec(memory_space=pltpu.VMEM)
    smem = pl.BlockSpec(memory_space=pltpu.SMEM)
    anywhere = pl.BlockSpec(memory_space=pl.ANY)
    dma = pltpu.SemaphoreType.DMA
    scratch = [
        pltpu.VMEM((64, 64, 128), F32),
        pltpu.VMEM((64, 128, 128), B16),
        pltpu.VMEM((64, 128, 128), B16),
        pltpu.VMEM((64, 128, 128), F32),
        pltpu.VMEM((2, 256, 512), B16),
        pltpu.VMEM((2, 128, 256), B16),
        pltpu.VMEM((2, 256, 1024), B16),
        pltpu.VMEM((2, 1024, 256), B16),
        pltpu.VMEM((64, 128), F32),
        pltpu.VMEM((64, 128), F32),
        pltpu.VMEM((64, 128), F32),
        pltpu.VMEM((8, 64, 256), B16),
        pltpu.VMEM((8, 2, 64, 512), B16),
        pltpu.VMEM((4, 4, 64, 512), B16),
        pltpu.VMEM((4, 2, 64, 512), B16),
        pltpu.VMEM((6, 64, 512), B16),
        pltpu.VMEM((4, 64, 512), B16),
        pltpu.VMEM((64, 128), F32),
        pltpu.VMEM((64, 128), F32),
        pltpu.VMEM((64, 128), B16),
        pltpu.VMEM((8, 2, 64, 128), B16),
        pltpu.VMEM((8, 64, 256), B16),
        pltpu.VMEM((8, 64, 256), B16),
        pltpu.VMEM((2, 8, 64), F32),
        pltpu.VMEM((16, 2, 8, 64), F32),
        pltpu.VMEM((3, 8, 64), F32),
        pltpu.VMEM((3, 8, 64), F32),
        pltpu.VMEM((1, 2048), F32),
        pltpu.VMEM((16, 1, 2048), F32),
        pltpu.VMEM((32, 256), F32),
        pltpu.VMEM((32, 2048), F32),
        pltpu.VMEM((64, 256), B16),
        pltpu.VMEM((64, 256), B16),
        pltpu.VMEM((8, 64, 256), B16),
        pltpu.VMEM((2, 4, 4, 32, 1024), B16),
        pltpu.VMEM((2, 4, 4, 32, 1024), B16),
        pltpu.VMEM((2, 4, 32, 1024), B16),
        pltpu.VMEM((2, 4, 32, 1024), B16),
        pltpu.VMEM((2, 32, 1024), F32),
        pltpu.VMEM((2, 4, 4, 32, 1024), B16),
        pltpu.VMEM((2, 4, 4, 32, 256), F32),
        pltpu.VMEM((8, 64, 256), B16),
        pltpu.VMEM((8, 64, 256), B16),
        pltpu.VMEM((2, 8, 64), F32),
        pltpu.VMEM((16, 2, 8, 64), F32),
        dma((10,)),
        dma((200,)),
        dma((7,)),
        dma((8,)),
        dma((4, 4)),
        dma((4, 2)),
        dma((4,)),
        dma((8, 2)),
        dma((8,)),
        dma((16,)),
        dma((1,)),
        dma((16,)),
        dma((8,)),
        dma((2, 4, 4)),
        dma((2, 4)),
        dma((2, 4)),
        dma((2, 4, 4)),
        dma((8,)),
        dma((16,)),
    ]
    return pl.pallas_call(
        kernel,
        out_shape=jax.ShapeDtypeStruct((64, 256), B16),
        in_specs=[vmem] * 5 + [smem] + [anywhere] * 10,
        out_specs=vmem,
        scratch_shapes=scratch,
        name="layer",
        compiler_params=pltpu.CompilerParams(
            collective_id=0, has_side_effects=True, vmem_limit_bytes=56 * 1024 * 1024
        ),
    )(
        tokens, lengths[None, :], head_gain[None, :], mixer_gain[None, :], final_gain[None, :], decay_rate,
        state_block, cached_keys, cached_values, query_weight, key_weight, value_weight, gate_weight,
        out_weight, up_weight, down_weight,
    )


def solution(mesh):
    finer = Mesh(mesh.devices.reshape(4, 4, 8, 2), AXES)
    kv, tp = ("y", "x"), ("z", "c")
    placed = (
        P(tp, kv), P(kv), P(kv, None, tp), P(kv, None, tp), P(kv, None, tp),
        P(kv, tp), P(kv, tp), P(kv, tp), P(kv, tp), P(tp), P(tp), P(tp, kv), P(kv),
        P(kv, tp), P(tp, kv), P(kv),
    )
    return jax.shard_map(per_device, mesh=finer, in_specs=placed, out_specs=P(tp, kv), check_vma=False)
```

time: 114 us -> 107 us (0.939); the launches traced: 114 us -> 106 us
  Pallas kernels: 109 us -> 104 us
  local copies, waits for them, and re-layouts: 3.44 us -> 1.38 us
  other arithmetic: 1.69 us -> 0 us
    pallas_call x1, Pallas kernels: 109 us -> 104 us  [per_device(): pl.pallas_call(kernel, out_shape=jax.ShapeDtypeStruct((64, 256), B16), in...]
    broadcast_in_dim x2 -> x0, local copies, waits for them, and re-layouts: 1.4 us -> none  [the longest x1 0.72 us: per_device(): rate = jnp.repeat(decay_rate, HDIM)[None, :]]
where the time goes in v3:
time: 107 us; the launch traced here: 106 us
  Pallas kernels  104 us (97%)
  local copies, waits for them, and re-layouts  1.38 us (1%)
    pallas_call x1, Pallas kernels, per_device(): pl.pallas_call(kernel, out_shape=jax.ShapeDtypeStruct((64, 256), B16), in...  104 us

profile of v3, /device:TPU:2, one launch (start us, length us, event | category | flops | bytes accessed | tf_op | source)
XLA Modules:
  0.0 105.8 jit_solution(17364072193605332035)
XLA Ops:
  0.0 104.4 %layer.1 = bf16[64,256]{1,0:T(8,128)(2,1)} custom-call(bf16[64,256]{1,0:T(8,128)(2,1)} %tok.1, s32[1,64]{1,0:T(1,128)} %bitcast.6, f32[1,128]{1,0:T(1,128)} %bitcast.7, f32[1,256]{1,0:T(1,128)} %bitcast.4, f32[1,256]{1,0:T(1,128)} %bitcast.5, f32[2]{0:T(128)} %rates.1, f32[64,64,128]{2,1,0:T(8,128)} %state_h.1, bf16[64,128,128]{2,1,0:T(8,128)(2,1)} %keys_h.1, ...), custom_call_target="tpu_custom_call" | custom-call | tf_op jit(solution)/shard_map/layer/pallas_call | solution.py:614
  104.4 1.4 %copy.18 = bf16[64,256]{1,0:T(8,128)(2,1)} copy(bf16[64,256]{1,0:T(8,128)(2,1)} %layer.1) | data formatting | bytes 65536

commit v4 on v3

--- a/solution.py
+++ b/solution.py
@@ -51,14 +51,17 @@
     state, keys, values, factor, wp, wo, wu, wd, cosine, sine, offset,
     t_all, b1_out, b1_in0, b1_in1, b2_out, b2_in, retained, turned, heads, m_all, d_out, d_in,
     s_out, s_in, p_out, p_in, col_out, col_in, ends, lift, payload, hidden, h_all,
-    g1_out, g1_in, g2_out, g2_in, g_sum, act_all, e_sum, e_out, e_in, j_out, j_in,
-    local, send, r_w, r_a, r_b10, r_b11, r_b2, r_c, r_d, r_e, r_p, r_col, r_f, r_g1, r_g2, r_h1, r_h2, r_i, r_j,
+    g1_out, g1_inx, g1_iny, g2_out, g2_in, g_sum, act_all, e_out, e_in, j_out, j_in,
+    local, send, r_w, r_a, r_b10, r_b11, r_b2, r_c, r_d, r_e, r_p, r_col, r_f,
+    r_g1x, r_g1y, r_g2, r_h1, r_h2, r_i, r_j, r_x, r_v,
 ):
     y, x, z, c = [lax.axis_index(name) for name in AXES]
     kv = y * 4 + x
     sibling = (y, x, z, 1 - c)
     row_of = lax.rem(x, 2)
     owner = row_of == c
+    pair = x // 2
+    partner = (y, 2 * pair + 1 - row_of, z, c)
     used = [0]
     pending = []
 
@@ -108,8 +111,8 @@
     for src, dst in zip((wq_h, wk_h, wv_h, wg_h), quarter):
         fetch(src, dst)
     fetch(wo_h, wo.at[c])
-    fetch(wu_h, wu.at[c])
-    fetch(wd_h, wd.at[c])
+    fetch(wu_h, wu.at[row_of, c])
+    fetch(wd_h, wd.at[row_of, c])
     fetch(keys_h, keys)
     fetch(values_h, values)
     fetch(state_h, state)
@@ -127,6 +130,9 @@
         peer = (y, x, lax.rem(z + dz, 8), c)
         pl.semaphore_signal(barrier, inc=1, device_id=peer, device_id_type=pl.DeviceIdType.MESH)
         greeted += 1
+        peer = (y, 2 * pair + 1 - row_of, lax.rem(z + dz, 8), c)
+        pl.semaphore_signal(barrier, inc=1, device_id=peer, device_id_type=pl.DeviceIdType.MESH)
+        greeted += 1
 
     ones = jnp.full((8, 256), 1.0, B16)
     first = jnp.where(lax.broadcasted_iota(jnp.int32, (8, 256), 0) == 0, 1.0, 0.0).astype(B16)
@@ -143,6 +149,20 @@
             term = lax.dot_general(ones, part, (((1,), (1,)), ((), ())), preferred_element_type=F32)
             total = term if total is None else total + term
         return total
+
+    def packed_sums(part_mean, part_centred):
+        means = jnp.broadcast_to(part_mean * (1.0 / 256), (64, 256))
+        return row_sums(jnp.concatenate([means, part_centred * part_centred], 0))
+
+    def combined(own_sums, sums):
+        total = jnp.sum(sums[...], axis=0)
+        mean = total * (1.0 / 16)
+        shift = jnp.where((lane_row < 64)[None], sums[...] - mean[None], 0.0)
+        between = jnp.sum(shift * shift, axis=0)
+        spread = (pltpu.roll(total, 64, 1) + 256.0 * between) * (1.0 / 4096)
+        scale = jnp.where(lane_row < 64, lax.rsqrt(spread + EPS), 0.0)
+        own_shift = jnp.broadcast_to(jnp.where(lane_row < 64, own_sums[...] - mean, 0.0), (8, 128))
+        return shift, own_shift, jnp.broadcast_to(scale, (8, 128))
 
     def column(u):
         total = None
@@ -178,10 +198,25 @@
     for d in NEAR[1:]:
         put(tok, t_all.at[z], r_a.at[z], (y, x, lax.rem(z + d, 8), c))
     for i, (src, dst) in enumerate(
-        [*zip((wq_h, wk_h, wv_h, wg_h), quarter), (wo_h, wo.at[c]), (wu_h, wu.at[c]), (wd_h, wd.at[c])]
+        [*zip((wq_h, wk_h, wv_h, wg_h), quarter), (wo_h, wo.at[c])]
     ):
         put(src, dst, r_w.at[i], sibling)
-    theirs = [wp.at[1 - c, :, pl.ds(128 * i, 128)] for i in range(4)] + [w.at[1 - c] for w in (wo, wu, wd)]
+    theirs = [wp.at[1 - c, :, pl.ds(128 * i, 128)] for i in range(4)]
+    theirs += [wo.at[1 - c], wu.at[row_of, 1 - c], wd.at[row_of, 1 - c]]
+    def chunk(k, side, core):
+        if k < 2:
+            return wu.at[side, core, pl.ds(128 * k, 128), :]
+        return wd.at[side, core, pl.ds(512 * (k - 2), 512), :]
+
+    def to_partner(k):
+        put(chunk(k, row_of, c), chunk(k, row_of, c), r_x.at[k], partner)
+
+    def on_to_sibling(k):
+        arrived(chunk(k, 1 - row_of, c), r_x.at[k])
+        put(chunk(k, 1 - row_of, c), chunk(k, 1 - row_of, c), r_v.at[k], sibling)
+
+    here[5].wait()
+    to_partner(0)
     for i in range(4):
         here[i].wait()
         arrived(theirs[i], r_w.at[i])
@@ -207,6 +242,9 @@
 
             put(b1_out.at[zp, colour], dst, sem, to, jnp.logical_not(mine))
 
+    put(wu_h, wu.at[row_of, c], r_w.at[5], sibling)
+    put(wd_h, wd.at[row_of, c], r_w.at[6], sibling)
+
     def first_stage_x(j):
         piece = lax.rem(z // 2 + j, 4)
 
@@ -257,12 +295,13 @@
     first_stage_y(1)
     first_stage_x(2)
 
+    here[6].wait()
+    to_partner(1)
     for i in (5, 6):
-        here[i].wait()
         arrived(theirs[i], r_w.at[i])
     gain_rows = jnp.broadcast_to(mixer_gain[...], (8, 256))
     for half in range(2):
-        col_out[:, pl.ds(1024 * half, 1024)] = split_dot(gain_rows, wu[half], 3)[0:1]
+        col_out[:, pl.ds(1024 * half, 1024)] = split_dot(gain_rows, wu[row_of, half], 3)[0:1]
     col_in[kv] = col_out[...]
     for k in (5, 7, 13, 15, 6, 14, 9, 11, 10, 1, 4, 3, 12, 2, 8):
         to = (lax.rem(y + k // 4, 4), lax.rem(x + k % 4, 4), z, c)
@@ -300,8 +339,8 @@
     def attend(i, carry):
         rows = pl.ds(pl.multiple_of(i * 8, 8), 8)
         q = turned[rows, :]
-        products = (keys[rows].astype(F32) * q[:, None, :]).reshape(8 * BLK, 128)
-        scores = split_dot(products, same_head, 2).reshape(8, BLK, 128)
+        products = (keys[rows] * q.astype(B16)[:, None, :]).reshape(8 * BLK, 128)
+        scores = dot(products, same_head).reshape(8, BLK, 128)
         weights = (scores * factor[rows]).astype(B16).astype(F32)
         inner = jnp.sum(weights * values[rows].astype(F32), axis=1)
         spread = (q[:, None, :] * pick[None]).reshape(8 * HDIM, 128).astype(B16)
@@ -327,6 +366,10 @@
     @pl.when(owner)
     def _():
         m_all[half, c] = mixed
+
+    for k in range(2, 4):
+        to_partner(k)
+    on_to_sibling(0)
 
     here[4].wait()
     arrived(theirs[4], r_w.at[4])
@@ -348,6 +391,7 @@
 
         d_out[i] = part
         put(d_out.at[i], d_in.at[z], r_d.at[z], (y, x, i, c), jnp.logical_not(mine))
+    on_to_sibling(1)
     branch = d_in[z].astype(F32)
     for d in NEAR[1:]:
         i = lax.rem(z + 8 - d, 8)
@@ -359,56 +403,66 @@
     part_centred = tall - part_mean
     scaled = (part_centred * mixer_gain[...]).astype(B16)
     payload[...] = scaled
-    h_all[z] = scaled
-    for d in (4, 3, 5, 2, 6, 1, 7):
-        put(payload, h_all.at[z], r_f.at[z], (y, x, lax.rem(z + d, 8), c))
-    s_out[0] = row_sums(jnp.broadcast_to(part_mean, (64, 256))) * (1.0 / 256)
-    s_out[1] = row_sums(part_centred * part_centred)
+    turn = lax.rem(z, 2)
+    stays = turn == row_of
+
+    @pl.when(stays)
+    def _():
+        h_all[z // 2, row_of] = scaled
+
+    for d in (4, 3, 5, 2, 6, 1, 7, 0):
+        put(
+            payload, h_all.at[z // 2, row_of], r_f.at[z // 2, row_of],
+            (y, 2 * pair + turn, lax.rem(z + d, 8), c), None if d else jnp.logical_not(stays),
+        )
+    s_out[...] = packed_sums(part_mean, part_centred)[0:1]
     s_in[kv] = s_out[...]
     for k in (10, 5, 7, 13, 15, 6, 14, 9, 11, 1, 4, 3, 12, 2, 8):
         to = (lax.rem(y + k // 4, 4), lax.rem(x + k % 4, 4), z, c)
         put(s_out, s_in.at[kv], r_e.at[kv], to)
 
-    along = (x, y)
+    for k in range(2):
+        arrived(chunk(k, 1 - row_of, 1 - c), r_v.at[k])
+
+    along = (pair, y)
+    size = (2, 4)
 
     def device_on(colour, stage, index):
         if (colour + stage) % 2 == 0:
-            return (y, index, z, c)
+            return (y, 2 * index + row_of, z, c)
         return (index, x, z, c)
 
-    for d in NEAR:
-        zp = lax.rem(z + 8 - d, 8)
-        if d:
-            arrived(h_all.at[zp], r_f.at[zp])
-        yd, xd = zp // 2, lax.rem(zp, 2) * 2
-        rows = h_all[zp]
+    for d in range(4):
+        t = lax.rem(z // 2 + (0, 1, 3, 2)[d], 4)
+        for side in range(2):
+            here_already = jnp.logical_and(2 * t + row_of == z, row_of == side)
+            arrived(h_all.at[t, side], r_f.at[t, side], jnp.logical_not(here_already))
         for colour in range(2):
-            part = dot(rows, wu[colour]).astype(B16)
+            part = (dot(h_all[t, 0], wu[0, colour]) + dot(h_all[t, 1], wu[1, colour])).astype(B16)
             for side in range(2):
-                rows_of = part[32 * side : 32 * side + 32]
-                me, to, piece = (x, xd + side, yd) if colour == 0 else (y, yd, xd + side)
-                g1_out[colour, to, piece] = rows_of
-                put(
-                    g1_out.at[colour, to, piece], g1_in.at[colour, me, piece],
-                    r_g1.at[colour, me, piece], device_on(colour, 0, to), to != me,
-                )
+                g1_out[colour, t, side] = part[32 * side : 32 * side + 32]
+                spot = g1_out.at[colour, t, side]
+                if colour == 0:
+                    put(
+                        spot, g1_inx.at[pair, t], r_g1x.at[pair, t], device_on(0, 0, side),
+                        pair != side,
+                    )
+                else:
+                    put(spot, g1_iny.at[y, side], r_g1y.at[y, side], device_on(1, 0, t), y != t)
 
     for k in (1, 4, 3, 12, 2, 8, 5, 7, 13, 15, 6, 14, 9, 11, 10):
         i = lax.rem(y + k // 4, 4) * 4 + lax.rem(x + k % 4, 4)
         arrived(s_in.at[i], r_e.at[i])
-    means = s_in[:, 0]
-    mean = jnp.sum(means, axis=0) * (1.0 / 16)
-    shift = means - mean[None]
-    spread = (jnp.sum(s_in[:, 1], axis=0) + 256.0 * jnp.sum(shift * shift, axis=0)) * (1.0 / 4096)
-    scale = lax.rsqrt(spread + EPS)
-    eight = lax.broadcasted_iota(jnp.int32, (8, 64), 0)
+    shift, own_shift, scale = combined(s_out, s_in)
+    eight = lax.broadcasted_iota(jnp.int32, (8, 128), 0)
     for group in range(2):
-        stacked = jnp.zeros((8, 64), F32)
+        stacked = jnp.zeros((8, 128), F32)
         for k in range(8):
             stacked = jnp.where(eight == k, shift[8 * group + k], stacked)
         p_out[group] = stacked
     p_out[2] = scale
-    mine = half == z
+    ends_at = 2 * y + row_of
+    mine = ends_at == z
 
     @pl.when(mine)
     def _():
@@ -416,15 +470,36 @@
 
     for d in range(1, 8):
         put(p_out, p_in, r_p.at[0], (y, x, lax.rem(z + d, 8), c), mine)
-    own_shift = s_out[0] - mean
-    hidden[...] = ((part_centred + column(own_shift)) * column(scale) * mixer_gain[...]).astype(B16)
+    wide_shift, wide_scale = column(own_shift)[:64], column(scale)[:64]
+    hidden[...] = ((part_centred + wide_shift) * wide_scale * mixer_gain[...]).astype(B16)
+
+    def first_sum(colour, j):
+        me, other = along[colour], along[1 - colour]
+        piece = lax.rem(other + j, size[1 - colour])
+        total = (g1_out[0, piece, me] if colour == 0 else g1_out[1, me, piece]).astype(F32)
+        for d in (1, 3, 2) if colour else (1,):
+            source = lax.rem(me + d, size[colour])
+            spot, sem = (g1_iny, r_g1y) if colour else (g1_inx, r_g1x)
+            arrived(spot.at[source, piece], sem.at[source, piece])
+            total = total + spot[source, piece].astype(F32)
+        if j:
+            g2_out[colour, piece] = total.astype(B16)
+            put(
+                g2_out.at[colour, piece], g2_in.at[colour, other], r_g2.at[colour, other],
+                device_on(colour, 1, piece),
+            )
+        else:
+            g_sum[colour] = total + lift[:, 1024 * colour : 1024 * colour + 1024]
+
+    for colour, j in ((0, 2), (1, 1), (0, 1), (0, 3)):
+        first_sum(colour, j)
 
     for k in range(1, 16):
         i = lax.rem(y + k // 4, 4) * 4 + lax.rem(x + k % 4, 4)
         arrived(col_in.at[i], r_col.at[i])
     wide_eight = lax.broadcasted_iota(jnp.int32, (8, 2048), 0)
     arrived(p_in, r_p.at[0], jnp.logical_not(mine))
-    lifted = jnp.zeros((64, 2048), F32)
+    lifted = jnp.zeros((128, 2048), F32)
     for group in range(2):
         stacked = jnp.zeros((8, 2048), F32)
         for k in range(8):
@@ -435,91 +510,89 @@
         col_low = (stacked - col_high.astype(F32)).astype(B16)
         for a, b in ((shift_high, col_high), (shift_high, col_low), (shift_low, col_high)):
             lifted = lifted + lax.dot_general(a, b, (((0,), (0,)), ((), ())), preferred_element_type=F32)
-    upper = row_of == 1
-    lift[...] = jnp.where(upper, lifted[32:], lifted[:32])
+    upper = pair == 1
+    lift[...] = jnp.where(upper, lifted[32:64], lifted[:32])
     scales = column(p_in[2])
-    ends[...] = jnp.where(upper, scales[32:], scales[:32])
-
-    for j in (0, 1, 3, 2):
-        for colour in range(2):
-            me, other = along[colour], along[1 - colour]
-            piece = lax.rem(other + j, 4)
-            total = g1_out[colour, me, piece].astype(F32)
-            for d in (1, 3, 2):
-                source = lax.rem(me + d, 4)
-                arrived(g1_in.at[colour, source, piece], r_g1.at[colour, source, piece])
-                total = total + g1_in[colour, source, piece].astype(F32)
-            if j:
-                g2_out[colour, piece] = total.astype(B16)
-                put(
-                    g2_out.at[colour, piece], g2_in.at[colour, other], r_g2.at[colour, other],
-                    device_on(colour, 1, piece),
-                )
-            else:
-                g_sum[colour] = total + lift[:, 1024 * colour : 1024 * colour + 1024]
-
-    def place(colour, i, j):
-        if colour == 0:
-            return (colour, i, j)
-        return (colour, j, i)
+    ends[...] = jnp.where(upper, scales[32:64], scales[:32])
+
+    for colour, j in ((0, 0), (1, 0)):
+        first_sum(colour, j)
+    for k in range(2, 4):
+        on_to_sibling(k)
+
+    def others(n):
+        return (2, 1, 3) if n == 4 else (1,)
 
     for colour in range(2):
         me, other = along[colour], along[1 - colour]
         total = g_sum[colour]
-        for d in (1, 3, 2):
-            source = lax.rem(other + d, 4)
+        for d in others(size[1 - colour]):
+            source = lax.rem(other + d, size[1 - colour])
             arrived(g2_in.at[colour, source], r_g2.at[colour, source])
             total = total + g2_in[colour, source].astype(F32)
         times = jnp.concatenate([ends[...]] * 4, 1)
         active = jnp.square(jnp.maximum(total * times, 0.0)).astype(B16)
-        spot = act_all.at[colour, y, x]
-        act_all[colour, y, x] = active
-        for d in (2, 1, 3):
-            put(spot, spot, r_h1.at[colour, other], device_on(colour, 1, lax.rem(other + d, 4)))
-        for d in (2, 1, 3):
-            put(spot, spot, r_h2.at[colour, other, me], device_on(colour, 0, lax.rem(me + d, 4)))
-    for j in (1, 3, 2):
+        spot = act_all.at[colour, y, pair]
+        act_all[colour, y, pair] = active
+        for stage in (1, 0):
+            at = along[colour] if stage == 0 else along[1 - colour]
+            n = size[(colour + stage) % 2]
+            sem = r_h2.at[colour, y, pair] if stage == 0 else r_h1.at[colour, other]
+            for d in others(n):
+                put(spot, spot, sem, device_on(colour, stage, lax.rem(at + d, n)))
+
+    def forward(colour, j):
+        me, other = along[colour], along[1 - colour]
+        source = lax.rem(other + j, size[1 - colour])
+        where = (source, pair) if colour == 0 else (y, source)
+        spot = act_all.at[colour, where[0], where[1]]
+        arrived(spot, r_h1.at[colour, source])
+        for d in others(size[colour]):
+            put(
+                spot, spot, r_h2.at[colour, where[0], where[1]],
+                device_on(colour, 0, lax.rem(me + d, size[colour])),
+            )
+
+    for colour, j in ((1, 1), (0, 1), (0, 3), (0, 2)):
+        forward(colour, j)
+
+    for k in range(2, 4):
+        arrived(chunk(k, 1 - row_of, 1 - c), r_v.at[k])
+
+    for j in (0, 1, 3, 2):
+        t = lax.rem(y + j, 4)
         for colour in range(2):
-            me, other = along[colour], along[1 - colour]
-            source = lax.rem(other + j, 4)
-            spot = act_all.at[place(colour, source, me)]
-            arrived(spot, r_h1.at[colour, source])
-            for d in (2, 1, 3):
-                put(spot, spot, r_h2.at[colour, source, me], device_on(colour, 0, lax.rem(me + d, 4)))
-
-    for j in (0, 1, 3, 2):
-        for colour in range(2):
-            me, other = along[colour], along[1 - colour]
-            source = lax.rem(other + j, 4)
-            for d in (1, 3, 2):
-                at = lax.rem(me + d, 4)
-                arrived(act_all.at[place(colour, source, at)], r_h2.at[colour, source, at])
-            if colour == 0:
-                rows = act_all[0, source].reshape(128, 1024)
-            else:
-                rows = act_all[1, :, source].reshape(128, 1024)
-            e_sum[colour, source] = dot(rows, wd[colour]).reshape(4, 32, 256)
-    for d in (4, 3, 5, 2, 6, 1, 7, 0):
-        i = lax.rem(z + d, 8)
-        yd, xd = i // 2, lax.rem(i, 2) * 2
-        part = jnp.concatenate(
-            [e_sum[0, yd, xd + side] + e_sum[1, xd + side, yd] for side in range(2)], 0
-        )
-        if d:
-            e_out[i] = part.astype(B16)
-            put(e_out.at[i], e_in.at[z], r_i.at[z], (y, x, i, c))
-        else:
-            downward = part
-    for d in NEAR[1:]:
+            for side in range(2):
+                if colour == 0:
+                    arrived(act_all.at[0, t, side], r_h2.at[0, t, side], pair != side)
+                elif j:
+                    arrived(act_all.at[1, t, side], r_h2.at[1, t, side])
+        upper_rows = act_all[0, t].reshape(64, 1024)
+        lower_rows = act_all[1, t].reshape(64, 1024)
+        for side in range(2):
+            part = (dot(upper_rows, wd[side, 0]) + dot(lower_rows, wd[side, 1])).astype(B16)
+            keep = jnp.logical_and(2 * t + row_of == z, row_of == side)
+            e_out[t, side] = part
+
+            @pl.when(keep)
+            def _():
+                e_in[z] = part
+
+            put(
+                e_out.at[t, side], e_in.at[z], r_i.at[z], (y, 2 * pair + side, 2 * t + row_of, c),
+                jnp.logical_not(keep),
+            )
+    downward = None
+    for d in NEAR:
         i = lax.rem(z + 8 - d, 8)
-        arrived(e_in.at[i], r_i.at[i])
-        downward = downward + e_in[i].astype(F32)
+        arrived(e_in.at[i], r_i.at[i], None if d else jnp.logical_not(stays))
+        term = e_in[i].astype(F32)
+        downward = term if downward is None else downward + term
 
     tall = ALPHA * hidden[...].astype(F32) + downward
     part_mean = jnp.sum(tall, axis=1, keepdims=True) * (1.0 / 256)
     part_centred = tall - part_mean
-    j_out[0] = row_sums(jnp.broadcast_to(part_mean, (64, 256))) * (1.0 / 256)
-    j_out[1] = row_sums(part_centred * part_centred)
+    j_out[...] = packed_sums(part_mean, part_centred)[0:1]
     j_in[kv] = j_out[...]
     for k in (10, 5, 7, 13, 15, 6, 14, 9, 11, 1, 4, 3, 12, 2, 8):
         to = (lax.rem(y + k // 4, 4), lax.rem(x + k % 4, 4), z, c)
@@ -527,12 +600,9 @@
     for k in range(1, 16):
         i = lax.rem(y + k // 4, 4) * 4 + lax.rem(x + k % 4, 4)
         arrived(j_in.at[i], r_j.at[i])
-    means = j_in[:, 0]
-    mean = jnp.sum(means, axis=0) * (1.0 / 16)
-    shift = means - mean[None]
-    spread = (jnp.sum(j_in[:, 1], axis=0) + 256.0 * jnp.sum(shift * shift, axis=0)) * (1.0 / 4096)
-    scale = lax.rsqrt(spread + EPS)
-    out[...] = ((part_centred + column(j_out[0] - mean)) * column(scale) * final_gain[...]).astype(B16)
+    shift, own_shift, scale = combined(j_out, j_in)
+    wide_shift, wide_scale = column(own_shift)[:64], column(scale)[:64]
+    out[...] = ((part_centred + wide_shift) * wide_scale * final_gain[...]).astype(B16)
     settle()
 
 
@@ -552,8 +622,8 @@
         pltpu.VMEM((64, 128, 128), F32),
         pltpu.VMEM((2, 256, 512), B16),
         pltpu.VMEM((2, 128, 256), B16),
-        pltpu.VMEM((2, 256, 1024), B16),
-        pltpu.VMEM((2, 1024, 256), B16),
+        pltpu.VMEM((2, 2, 256, 1024), B16),
+        pltpu.VMEM((2, 2, 1024, 256), B16),
         pltpu.VMEM((64, 128), F32),
         pltpu.VMEM((64, 128), F32),
         pltpu.VMEM((64, 128), F32),
@@ -569,28 +639,28 @@
         pltpu.VMEM((8, 2, 64, 128), B16),
         pltpu.VMEM((8, 64, 256), B16),
         pltpu.VMEM((8, 64, 256), B16),
-        pltpu.VMEM((2, 8, 64), F32),
-        pltpu.VMEM((16, 2, 8, 64), F32),
-        pltpu.VMEM((3, 8, 64), F32),
-        pltpu.VMEM((3, 8, 64), F32),
+        pltpu.VMEM((1, 128), F32),
+        pltpu.VMEM((16, 1, 128), F32),
+        pltpu.VMEM((3, 8, 128), F32),
+        pltpu.VMEM((3, 8, 128), F32),
         pltpu.VMEM((1, 2048), F32),
         pltpu.VMEM((16, 1, 2048), F32),
         pltpu.VMEM((32, 256), F32),
         pltpu.VMEM((32, 2048), F32),
         pltpu.VMEM((64, 256), B16),
         pltpu.VMEM((64, 256), B16),
-        pltpu.VMEM((8, 64, 256), B16),
-        pltpu.VMEM((2, 4, 4, 32, 1024), B16),
-        pltpu.VMEM((2, 4, 4, 32, 1024), B16),
+        pltpu.VMEM((4, 2, 64, 256), B16),
+        pltpu.VMEM((2, 4, 2, 32, 1024), B16),
+        pltpu.VMEM((2, 4, 32, 1024), B16),
+        pltpu.VMEM((4, 2, 32, 1024), B16),
         pltpu.VMEM((2, 4, 32, 1024), B16),
         pltpu.VMEM((2, 4, 32, 1024), B16),
         pltpu.VMEM((2, 32, 1024), F32),
-        pltpu.VMEM((2, 4, 4, 32, 1024), B16),
-        pltpu.VMEM((2, 4, 4, 32, 256), F32),
+        pltpu.VMEM((2, 4, 2, 32, 1024), B16),
+        pltpu.VMEM((4, 2, 64, 256), B16),
         pltpu.VMEM((8, 64, 256), B16),
-        pltpu.VMEM((8, 64, 256), B16),
-        pltpu.VMEM((2, 8, 64), F32),
-        pltpu.VMEM((16, 2, 8, 64), F32),
+        pltpu.VMEM((1, 128), F32),
+        pltpu.VMEM((16, 1, 128), F32),
         dma((10,)),
         dma((200,)),
         dma((7,)),
@@ -603,13 +673,16 @@
         dma((16,)),
         dma((1,)),
         dma((16,)),
-        dma((8,)),
-        dma((2, 4, 4)),
+        dma((4, 2)),
+        dma((2, 4)),
+        dma((4, 2)),
         dma((2, 4)),
         dma((2, 4)),
-        dma((2, 4, 4)),
+        dma((2, 4, 2)),
         dma((8,)),
         dma((16,)),
+        dma((4,)),
+        dma((4,)),
     ]
     return pl.pallas_call(
         kernel,

time: 107 us -> 102 us (0.953)
  Pallas kernels: 104 us -> 99.5 us
    pallas_call x1, Pallas kernels: 104 us -> 99.5 us  [per_device(): pl.pallas_call(kernel, out_shape=jax.ShapeDtypeStruct((64, 256), B16), in...]
where the time goes in v4:
time: 102 us; the launch traced here: 101 us
  Pallas kernels  99.5 us (98%)
  local copies, waits for them, and re-layouts  1.38 us (1%)
    pallas_call x1, Pallas kernels, per_device(): pl.pallas_call(kernel, out_shape=jax.ShapeDtypeStruct((64, 256), B16), in...  99.5 us

profile of v4, /device:TPU:2, one launch (start us, length us, event | category | flops | bytes accessed | tf_op | source)
XLA Modules:
  0.0 100.9 jit_solution(7398741294680784879)
XLA Ops:
  0.0 99.5 %layer.1 = bf16[64,256]{1,0:T(8,128)(2,1)} custom-call(bf16[64,256]{1,0:T(8,128)(2,1)} %tok.1, s32[1,64]{1,0:T(1,128)} %bitcast.6, f32[1,128]{1,0:T(1,128)} %bitcast.7, f32[1,256]{1,0:T(1,128)} %bitcast.4, f32[1,256]{1,0:T(1,128)} %bitcast.5, f32[2]{0:T(128)} %rates.1, f32[64,64,128]{2,1,0:T(8,128)} %state_h.1, bf16[64,128,128]{2,1,0:T(8,128)(2,1)} %keys_h.1, ...), custom_call_target="tpu_custom_call" | custom-call | tf_op jit(solution)/shard_map/layer/pallas_call | solution.py:687
  99.5 1.4 %copy.18 = bf16[64,256]{1,0:T(8,128)(2,1)} copy(bf16[64,256]{1,0:T(8,128)(2,1)} %layer.1) | data formatting | bytes 65536

commit v5 on v4

--- a/solution.py
+++ b/solution.py
@@ -14,6 +14,8 @@
 EPS = 1e-05
 AXES = ("y", "x", "z", "c")
 NEAR = (0, 1, 7, 2, 6, 3, 5, 4)
+POOL = 32
+SENDS = 36
 F32 = jnp.float32
 B16 = jnp.bfloat16
 
@@ -45,10 +47,10 @@
 
 
 def kernel(
-    tok, lengths, head_gain, mixer_gain, final_gain, rates,
+    tok_h, lengths_h, head_gain_h, mixer_gain_h, final_gain_h, rates,
     state_h, keys_h, values_h, wq_h, wk_h, wv_h, wg_h, wo_h, wu_h, wd_h,
     out,
-    state, keys, values, factor, wp, wo, wu, wd, cosine, sine, offset,
+    tok, lengths, head_gain, mixer_gain, final_gain, state, keys, values, factor, wp, wo, wu, wd, cosine, sine, offset,
     t_all, b1_out, b1_in0, b1_in1, b2_out, b2_in, retained, turned, heads, m_all, d_out, d_in,
     s_out, s_in, p_out, p_in, col_out, col_in, ends, lift, payload, hidden, h_all,
     g1_out, g1_inx, g1_iny, g2_out, g2_in, g_sum, act_all, e_out, e_in, j_out, j_in,
@@ -62,12 +64,28 @@
     owner = row_of == c
     pair = x // 2
     partner = (y, 2 * pair + 1 - row_of, z, c)
+    pending = [None] * SENDS
     used = [0]
-    pending = []
-
-    def put(src, dst, recv, device, when=None):
-        copy = copy_to(src, dst, send.at[used[0]], recv, device)
-        used[0] += 1
+
+    def sent(slot):
+        if pending[slot] is None:
+            return
+        when, copy = pending[slot]
+        pending[slot] = None
+        if when is None:
+            copy.wait_send()
+        else:
+
+            @pl.when(when)
+            def _():
+                copy.wait_send()
+
+    def put(src, dst, recv, device, when=None, slot=None):
+        if slot is None:
+            slot = used[0] % POOL
+            used[0] += 1
+        sent(slot)
+        copy = copy_to(src, dst, send.at[slot], recv, device)
         if when is None:
             copy.start()
         else:
@@ -76,20 +94,11 @@
             def _():
                 copy.start()
 
-        pending.append((when, copy))
+        pending[slot] = (when, copy)
 
     def settle():
-        for when, copy in pending:
-            if when is None:
-                copy.wait_send()
-            else:
-
-                @pl.when(when)
-                def _():
-                    copy.wait_send()
-
-        pending.clear()
-        used[0] = 0
+        for slot in range(SENDS):
+            sent(slot)
 
     def arrived(dst, sem, when=None):
         copy = copy_to(dst, dst, send.at[0], sem, sibling)
@@ -100,22 +109,6 @@
             @pl.when(when)
             def _():
                 copy.wait_recv()
-
-    here = []
-
-    def fetch(src, dst):
-        here.append(pltpu.make_async_copy(src, dst, local.at[len(here)]))
-        here[-1].start()
-
-    quarter = [wp.at[c, :, pl.ds(128 * i, 128)] for i in range(4)]
-    for src, dst in zip((wq_h, wk_h, wv_h, wg_h), quarter):
-        fetch(src, dst)
-    fetch(wo_h, wo.at[c])
-    fetch(wu_h, wu.at[row_of, c])
-    fetch(wd_h, wd.at[row_of, c])
-    fetch(keys_h, keys)
-    fetch(values_h, values)
-    fetch(state_h, state)
 
     barrier = pltpu.get_barrier_semaphore()
     greeted = 0
@@ -134,6 +127,30 @@
         pl.semaphore_signal(barrier, inc=1, device_id=peer, device_id_type=pl.DeviceIdType.MESH)
         greeted += 1
 
+    small = []
+    for src, dst in (
+        (lengths_h, lengths), (tok_h, tok), (head_gain_h, head_gain), (mixer_gain_h, mixer_gain),
+        (final_gain_h, final_gain),
+    ):
+        small.append(pltpu.make_async_copy(src, dst, local.at[10 + len(small)]))
+        small[-1].start()
+
+    here = []
+
+    def fetch(src, dst):
+        here.append(pltpu.make_async_copy(src, dst, local.at[len(here)]))
+        here[-1].start()
+
+    quarter = [wp.at[c, :, pl.ds(128 * i, 128)] for i in range(4)]
+    for src, dst in zip((wq_h, wk_h, wv_h, wg_h), quarter):
+        fetch(src, dst)
+    fetch(wo_h, wo.at[c])
+    fetch(wu_h, wu.at[row_of, c])
+    fetch(wd_h, wd.at[row_of, c])
+    fetch(keys_h, keys)
+    fetch(values_h, values)
+    fetch(state_h, state)
+
     ones = jnp.full((8, 256), 1.0, B16)
     first = jnp.where(lax.broadcasted_iota(jnp.int32, (8, 256), 0) == 0, 1.0, 0.0).astype(B16)
     lane = lax.broadcasted_iota(jnp.int32, (64, 128), 1)
@@ -173,6 +190,7 @@
             total = term if total is None else total + term
         return total
 
+    small[0].wait()
     position = column(jnp.broadcast_to(lengths[...].astype(F32), (8, 64)))[:, :128]
     offset[...] = position - jnp.floor(position * (1.0 / BLK)) * BLK
     inverse = jnp.zeros((1, 128), F32)
@@ -192,6 +210,8 @@
         return carry
 
     lax.fori_loop(0, 8, decay, 0)
+    for copy in small[1:]:
+        copy.wait()
     t_all[z] = tok[...]
     pl.semaphore_wait(barrier, greeted)
 
@@ -200,16 +220,15 @@
     for i, (src, dst) in enumerate(
         [*zip((wq_h, wk_h, wv_h, wg_h), quarter), (wo_h, wo.at[c])]
     ):
-        put(src, dst, r_w.at[i], sibling)
-    theirs = [wp.at[1 - c, :, pl.ds(128 * i, 128)] for i in range(4)]
-    theirs += [wo.at[1 - c], wu.at[row_of, 1 - c], wd.at[row_of, 1 - c]]
+        put(src, dst, r_w.at[max(i - 3, 0)], sibling)
+    theirs = [wp.at[1 - c], wo.at[1 - c], wu.at[row_of, 1 - c], wd.at[row_of, 1 - c]]
     def chunk(k, side, core):
         if k < 2:
             return wu.at[side, core, pl.ds(128 * k, 128), :]
         return wd.at[side, core, pl.ds(512 * (k - 2), 512), :]
 
     def to_partner(k):
-        put(chunk(k, row_of, c), chunk(k, row_of, c), r_x.at[k], partner)
+        put(chunk(k, row_of, c), chunk(k, row_of, c), r_x.at[k], partner, slot=POOL + k)
 
     def on_to_sibling(k):
         arrived(chunk(k, 1 - row_of, c), r_x.at[k])
@@ -219,7 +238,7 @@
     to_partner(0)
     for i in range(4):
         here[i].wait()
-        arrived(theirs[i], r_w.at[i])
+    arrived(theirs[0], r_w.at[0])
 
     for d in NEAR:
         zp = lax.rem(z + 8 - d, 8)
@@ -232,9 +251,9 @@
             part = dot(rows, wp[colour]).astype(B16)
             b1_out[zp, colour] = part
             if colour == 0:
-                mine, dst, sem, to = xd == x, b1_in0.at[x, yd], r_b10.at[x, yd], (y, xd, z, c)
+                mine, dst, sem, to = xd == x, b1_in0.at[x, yd], r_b10.at[yd], (y, xd, z, c)
             else:
-                mine, dst, sem, to = yd == y, b1_in1.at[y, side], r_b11.at[y, side], (yd, x, z, c)
+                mine, dst, sem, to = yd == y, b1_in1.at[y, side], r_b11.at[side], (yd, x, z, c)
 
             @pl.when(mine)
             def _():
@@ -242,17 +261,15 @@
 
             put(b1_out.at[zp, colour], dst, sem, to, jnp.logical_not(mine))
 
-    put(wu_h, wu.at[row_of, c], r_w.at[5], sibling)
-    put(wd_h, wd.at[row_of, c], r_w.at[6], sibling)
+    put(wu_h, wu.at[row_of, c], r_w.at[2], sibling)
+    put(wd_h, wd.at[row_of, c], r_w.at[3], sibling)
 
     def first_stage_x(j):
         piece = lax.rem(z // 2 + j, 4)
 
         @pl.when(owner)
         def _():
-            for k in (1, 3, 2):
-                i = lax.rem(x + k, 4)
-                arrived(b1_in0.at[i, piece], r_b10.at[i, piece])
+            arrived(b1_in0.at[pl.ds(0, 3), piece], r_b10.at[piece])
             total = b1_in0[0, piece].astype(F32)
             for k in range(1, 4):
                 total = total + b1_in0[k, piece].astype(F32)
@@ -265,15 +282,13 @@
             b2_in[y] = b2_out[j]
 
         put(
-            b2_out.at[j], b2_in.at[y], r_b2.at[y], (piece, x, z, 0),
+            b2_out.at[j], b2_in.at[y], r_b2.at[0], (piece, x, z, 0),
             jnp.logical_and(owner, jnp.logical_not(mine)),
         )
 
     def first_stage_y(j):
         side = lax.rem(z + j, 2)
-        for k in (1, 3, 2):
-            i = lax.rem(y + k, 4)
-            arrived(b1_in1.at[i, side], r_b11.at[i, side])
+        arrived(b1_in1.at[pl.ds(0, 3), side], r_b11.at[side])
         total = b1_in1[0, side].astype(F32)
         for k in range(1, 4):
             total = total + b1_in1[k, side].astype(F32)
@@ -286,7 +301,7 @@
         def _():
             b2_in[x] = total
 
-        put(b2_out.at[4 + j], b2_in.at[x], r_b2.at[x], (y, xd, z, 1), jnp.logical_not(mine))
+        put(b2_out.at[4 + j], b2_in.at[x], r_b2.at[0], (y, xd, z, 1), jnp.logical_not(mine))
 
     first_stage_x(0)
     first_stage_x(1)
@@ -297,7 +312,7 @@
 
     here[6].wait()
     to_partner(1)
-    for i in (5, 6):
+    for i in (2, 3):
         arrived(theirs[i], r_w.at[i])
     gain_rows = jnp.broadcast_to(mixer_gain[...], (8, 256))
     for half in range(2):
@@ -305,11 +320,10 @@
     col_in[kv] = col_out[...]
     for k in (5, 7, 13, 15, 6, 14, 9, 11, 10, 1, 4, 3, 12, 2, 8):
         to = (lax.rem(y + k // 4, 4), lax.rem(x + k % 4, 4), z, c)
-        put(col_out, col_in.at[kv], r_col.at[kv], to)
-
-    place_b2 = jnp.where(c == 0, y, x)
-    for k in range(4):
-        arrived(b2_in.at[k], r_b2.at[k], jnp.logical_not(jnp.logical_and(owner, place_b2 == k)))
+        put(col_out, col_in.at[kv], r_col.at[0], to)
+
+    arrived(b2_in.at[pl.ds(0, 3)], r_b2.at[0], owner)
+    arrived(b2_in, r_b2.at[0], jnp.logical_not(owner))
     qkvg = b2_in[0].astype(F32)
     for k in range(1, 4):
         qkvg = qkvg + b2_in[k].astype(F32)
@@ -361,7 +375,7 @@
 
     for k in (10, 5, 7, 13, 15, 6, 14, 9, 11, 1, 4, 3, 12, 2, 8, 0):
         to = (lax.rem(y + k // 4, 4), lax.rem(x + k % 4, 4), z, row_of)
-        put(heads, m_all.at[half, c], r_c.at[half, c], to, None if k else jnp.logical_not(owner))
+        put(heads, m_all.at[half, c], r_c.at[half], to, None if k else jnp.logical_not(owner))
 
     @pl.when(owner)
     def _():
@@ -372,16 +386,14 @@
     on_to_sibling(0)
 
     here[4].wait()
-    arrived(theirs[4], r_w.at[4])
+    arrived(theirs[1], r_w.at[1])
 
     start = 2 * y + x // 2
     for j in (0, 1, 7, 2, 6, 3, 5, 4):
         i = lax.rem(start + j, 8)
-        for core in range(2):
-            arrived(
-                m_all.at[i, core], r_c.at[i, core],
-                jnp.logical_not(jnp.logical_and(2 * i + c == kv, c == core)),
-            )
+        whole = 2 * i + c != kv
+        arrived(m_all.at[i], r_c.at[i], whole)
+        arrived(m_all.at[i, 0], r_c.at[i], jnp.logical_not(whole))
         part = (dot(m_all[i, 0], wo[0]) + dot(m_all[i, 1], wo[1])).astype(B16)
         mine = i == z
 
@@ -390,12 +402,12 @@
             d_in[i] = part
 
         d_out[i] = part
-        put(d_out.at[i], d_in.at[z], r_d.at[z], (y, x, i, c), jnp.logical_not(mine))
+        put(d_out.at[i], d_in.at[z], r_d.at[0], (y, x, i, c), jnp.logical_not(mine))
     on_to_sibling(1)
+    arrived(d_in.at[pl.ds(0, 7)], r_d.at[0])
     branch = d_in[z].astype(F32)
     for d in NEAR[1:]:
         i = lax.rem(z + 8 - d, 8)
-        arrived(d_in.at[i], r_d.at[i])
         branch = branch + d_in[i].astype(F32)
 
     tall = ALPHA * tok[...].astype(F32) + branch
@@ -412,14 +424,14 @@
 
     for d in (4, 3, 5, 2, 6, 1, 7, 0):
         put(
-            payload, h_all.at[z // 2, row_of], r_f.at[z // 2, row_of],
+            payload, h_all.at[z // 2, row_of], r_f.at[z // 2],
             (y, 2 * pair + turn, lax.rem(z + d, 8), c), None if d else jnp.logical_not(stays),
         )
     s_out[...] = packed_sums(part_mean, part_centred)[0:1]
     s_in[kv] = s_out[...]
     for k in (10, 5, 7, 13, 15, 6, 14, 9, 11, 1, 4, 3, 12, 2, 8):
         to = (lax.rem(y + k // 4, 4), lax.rem(x + k % 4, 4), z, c)
-        put(s_out, s_in.at[kv], r_e.at[kv], to)
+        put(s_out, s_in.at[kv], r_e.at[0], to)
 
     for k in range(2):
         arrived(chunk(k, 1 - row_of, 1 - c), r_v.at[k])
@@ -434,9 +446,9 @@
 
     for d in range(4):
         t = lax.rem(z // 2 + (0, 1, 3, 2)[d], 4)
-        for side in range(2):
-            here_already = jnp.logical_and(2 * t + row_of == z, row_of == side)
-            arrived(h_all.at[t, side], r_f.at[t, side], jnp.logical_not(here_already))
+        whole = 2 * t + row_of != z
+        arrived(h_all.at[t], r_f.at[t], whole)
+        arrived(h_all.at[t, 0], r_f.at[t], jnp.logical_not(whole))
         for colour in range(2):
             part = (dot(h_all[t, 0], wu[0, colour]) + dot(h_all[t, 1], wu[1, colour])).astype(B16)
             for side in range(2):
@@ -444,15 +456,13 @@
                 spot = g1_out.at[colour, t, side]
                 if colour == 0:
                     put(
-                        spot, g1_inx.at[pair, t], r_g1x.at[pair, t], device_on(0, 0, side),
+                        spot, g1_inx.at[pair, t], r_g1x.at[t], device_on(0, 0, side),
                         pair != side,
                     )
                 else:
-                    put(spot, g1_iny.at[y, side], r_g1y.at[y, side], device_on(1, 0, t), y != t)
-
-    for k in (1, 4, 3, 12, 2, 8, 5, 7, 13, 15, 6, 14, 9, 11, 10):
-        i = lax.rem(y + k // 4, 4) * 4 + lax.rem(x + k % 4, 4)
-        arrived(s_in.at[i], r_e.at[i])
+                    put(spot, g1_iny.at[y, side], r_g1y.at[side], device_on(1, 0, t), y != t)
+
+    arrived(s_in.at[pl.ds(0, 15)], r_e.at[0])
     shift, own_shift, scale = combined(s_out, s_in)
     eight = lax.broadcasted_iota(jnp.int32, (8, 128), 0)
     for group in range(2):
@@ -477,15 +487,17 @@
         me, other = along[colour], along[1 - colour]
         piece = lax.rem(other + j, size[1 - colour])
         total = (g1_out[0, piece, me] if colour == 0 else g1_out[1, me, piece]).astype(F32)
-        for d in (1, 3, 2) if colour else (1,):
-            source = lax.rem(me + d, size[colour])
-            spot, sem = (g1_iny, r_g1y) if colour else (g1_inx, r_g1x)
-            arrived(spot.at[source, piece], sem.at[source, piece])
-            total = total + spot[source, piece].astype(F32)
+        if colour == 0:
+            arrived(g1_inx.at[1 - pair, piece], r_g1x.at[piece])
+            total = total + g1_inx[1 - pair, piece].astype(F32)
+        else:
+            arrived(g1_iny.at[pl.ds(0, 3), piece], r_g1y.at[piece])
+            for d in (1, 3, 2):
+                total = total + g1_iny[lax.rem(y + d, 4), piece].astype(F32)
         if j:
             g2_out[colour, piece] = total.astype(B16)
             put(
-                g2_out.at[colour, piece], g2_in.at[colour, other], r_g2.at[colour, other],
+                g2_out.at[colour, piece], g2_in.at[colour, other], r_g2.at[colour],
                 device_on(colour, 1, piece),
             )
         else:
@@ -494,9 +506,7 @@
     for colour, j in ((0, 2), (1, 1), (0, 1), (0, 3)):
         first_sum(colour, j)
 
-    for k in range(1, 16):
-        i = lax.rem(y + k // 4, 4) * 4 + lax.rem(x + k % 4, 4)
-        arrived(col_in.at[i], r_col.at[i])
+    arrived(col_in.at[pl.ds(0, 15)], r_col.at[0])
     wide_eight = lax.broadcasted_iota(jnp.int32, (8, 2048), 0)
     arrived(p_in, r_p.at[0], jnp.logical_not(mine))
     lifted = jnp.zeros((128, 2048), F32)
@@ -526,9 +536,9 @@
     for colour in range(2):
         me, other = along[colour], along[1 - colour]
         total = g_sum[colour]
+        arrived(g2_in.at[colour, pl.ds(0, size[1 - colour] - 1)], r_g2.at[colour])
         for d in others(size[1 - colour]):
             source = lax.rem(other + d, size[1 - colour])
-            arrived(g2_in.at[colour, source], r_g2.at[colour, source])
             total = total + g2_in[colour, source].astype(F32)
         times = jnp.concatenate([ends[...]] * 4, 1)
         active = jnp.square(jnp.maximum(total * times, 0.0)).astype(B16)
@@ -537,7 +547,7 @@
         for stage in (1, 0):
             at = along[colour] if stage == 0 else along[1 - colour]
             n = size[(colour + stage) % 2]
-            sem = r_h2.at[colour, y, pair] if stage == 0 else r_h1.at[colour, other]
+            sem = r_h2.at[colour, y] if stage == 0 else r_h1.at[colour, other]
             for d in others(n):
                 put(spot, spot, sem, device_on(colour, stage, lax.rem(at + d, n)))
 
@@ -549,7 +559,7 @@
         arrived(spot, r_h1.at[colour, source])
         for d in others(size[colour]):
             put(
-                spot, spot, r_h2.at[colour, where[0], where[1]],
+                spot, spot, r_h2.at[colour, where[0]],
                 device_on(colour, 0, lax.rem(me + d, size[colour])),
             )
 
@@ -559,14 +569,11 @@
     for k in range(2, 4):
         arrived(chunk(k, 1 - row_of, 1 - c), r_v.at[k])
 
-    for j in (0, 1, 3, 2):
-        t = lax.rem(y + j, 4)
-        for colour in range(2):
-            for side in range(2):
-                if colour == 0:
-                    arrived(act_all.at[0, t, side], r_h2.at[0, t, side], pair != side)
-                elif j:
-                    arrived(act_all.at[1, t, side], r_h2.at[1, t, side])
+    for j in range(4):
+        t = y if j == 0 else j - 1 + (j - 1 >= y).astype(jnp.int32)
+        arrived(act_all.at[0, t, 0], r_h2.at[0, t])
+        if j:
+            arrived(act_all.at[1, t], r_h2.at[1, t])
         upper_rows = act_all[0, t].reshape(64, 1024)
         lower_rows = act_all[1, t].reshape(64, 1024)
         for side in range(2):
@@ -579,13 +586,14 @@
                 e_in[z] = part
 
             put(
-                e_out.at[t, side], e_in.at[z], r_i.at[z], (y, 2 * pair + side, 2 * t + row_of, c),
+                e_out.at[t, side], e_in.at[z], r_i.at[0], (y, 2 * pair + side, 2 * t + row_of, c),
                 jnp.logical_not(keep),
             )
+    arrived(e_in.at[pl.ds(0, 7)], r_i.at[0], stays)
+    arrived(e_in, r_i.at[0], jnp.logical_not(stays))
     downward = None
     for d in NEAR:
         i = lax.rem(z + 8 - d, 8)
-        arrived(e_in.at[i], r_i.at[i], None if d else jnp.logical_not(stays))
         term = e_in[i].astype(F32)
         downward = term if downward is None else downward + term
 
@@ -596,10 +604,8 @@
     j_in[kv] = j_out[...]
     for k in (10, 5, 7, 13, 15, 6, 14, 9, 11, 1, 4, 3, 12, 2, 8):
         to = (lax.rem(y + k // 4, 4), lax.rem(x + k % 4, 4), z, c)
-        put(j_out, j_in.at[kv], r_j.at[kv], to)
-    for k in range(1, 16):
-        i = lax.rem(y + k // 4, 4) * 4 + lax.rem(x + k % 4, 4)
-        arrived(j_in.at[i], r_j.at[i])
+        put(j_out, j_in.at[kv], r_j.at[0], to)
+    arrived(j_in.at[pl.ds(0, 15)], r_j.at[0])
     shift, own_shift, scale = combined(j_out, j_in)
     wide_shift, wide_scale = column(own_shift)[:64], column(scale)[:64]
     out[...] = ((part_centred + wide_shift) * wide_scale * final_gain[...]).astype(B16)
@@ -616,6 +622,11 @@
     anywhere = pl.BlockSpec(memory_space=pl.ANY)
     dma = pltpu.SemaphoreType.DMA
     scratch = [
+        pltpu.VMEM((64, 256), B16),
+        pltpu.VMEM((1, 64), jnp.int32),
+        pltpu.VMEM((1, 128), F32),
+        pltpu.VMEM((1, 256), F32),
+        pltpu.VMEM((1, 256), F32),
         pltpu.VMEM((64, 64, 128), F32),
         pltpu.VMEM((64, 128, 128), B16),
         pltpu.VMEM((64, 128, 128), B16),
@@ -661,33 +672,33 @@
         pltpu.VMEM((8, 64, 256), B16),
         pltpu.VMEM((1, 128), F32),
         pltpu.VMEM((16, 1, 128), F32),
-        dma((10,)),
-        dma((200,)),
-        dma((7,)),
+        dma((15,)),
+        dma((SENDS,)),
+        dma((4,)),
         dma((8,)),
-        dma((4, 4)),
-        dma((4, 2)),
         dma((4,)),
-        dma((8, 2)),
+        dma((2,)),
+        dma((1,)),
         dma((8,)),
-        dma((16,)),
         dma((1,)),
-        dma((16,)),
-        dma((4, 2)),
-        dma((2, 4)),
-        dma((4, 2)),
+        dma((1,)),
+        dma((1,)),
+        dma((1,)),
+        dma((4,)),
+        dma((4,)),
+        dma((2,)),
+        dma((2,)),
         dma((2, 4)),
         dma((2, 4)),
-        dma((2, 4, 2)),
-        dma((8,)),
-        dma((16,)),
+        dma((1,)),
+        dma((1,)),
         dma((4,)),
         dma((4,)),
     ]
     return pl.pallas_call(
         kernel,
         out_shape=jax.ShapeDtypeStruct((64, 256), B16),
-        in_specs=[vmem] * 5 + [smem] + [anywhere] * 10,
+        in_specs=[anywhere] * 5 + [smem] + [anywhere] * 10,
         out_specs=vmem,
         scratch_shapes=scratch,
         name="layer",

time: 102 us -> 99.8 us (0.978)
  Pallas kernels: 99.5 us -> 97 us
    pallas_call x1, Pallas kernels: 99.5 us -> 97 us  [per_device(): pl.pallas_call(kernel, out_shape=jax.ShapeDtypeStruct((64, 256), B16), in...]
where the time goes in v5:
time: 99.8 us; the launch traced here: 98.3 us
  Pallas kernels  97 us (97%)
  local copies, waits for them, and re-layouts  1.38 us (1%)
    pallas_call x1, Pallas kernels, per_device(): pl.pallas_call(kernel, out_shape=jax.ShapeDtypeStruct((64, 256), B16), in...  97 us

profile of v5, /device:TPU:2, one launch (start us, length us, event | category | flops | bytes accessed | tf_op | source)
XLA Modules:
  0.0 98.3 jit_solution(8030735005122122488)
XLA Ops:
  0.0 97.0 %layer.1 = bf16[64,256]{1,0:T(8,128)(2,1)} custom-call(bf16[64,256]{1,0:T(8,128)(2,1)} %tok_h.1, s32[1,64]{1,0:T(1,128)} %bitcast.6, f32[1,128]{1,0:T(1,128)} %bitcast.7, f32[1,256]{1,0:T(1,128)} %bitcast.4, f32[1,256]{1,0:T(1,128)} %bitcast.5, f32[2]{0:T(128)} %rates.1, f32[64,64,128]{2,1,0:T(8,128)} %state_h.1, bf16[64,128,128]{2,1,0:T(8,128)(2,1)} %keys_h.1, ...), custom_call_target="tpu_custom_call" | custom-call | tf_op jit(solution)/shard_map/layer/pallas_call | solution.py:698
  97.0 1.4 %copy.18 = bf16[64,256]{1,0:T(8,128)(2,1)} copy(bf16[64,256]{1,0:T(8,128)(2,1)} %layer.1) | data formatting | bytes 65536

commit v6 on v5

--- a/solution.py
+++ b/solution.py
@@ -215,7 +215,7 @@
     t_all[z] = tok[...]
     pl.semaphore_wait(barrier, greeted)
 
-    for d in NEAR[1:]:
+    for d in (1, 7, 2, 6):
         put(tok, t_all.at[z], r_a.at[z], (y, x, lax.rem(z + d, 8), c))
     for i, (src, dst) in enumerate(
         [*zip((wq_h, wk_h, wv_h, wg_h), quarter), (wo_h, wo.at[c])]
@@ -244,6 +244,8 @@
         zp = lax.rem(z + 8 - d, 8)
         if d:
             arrived(t_all.at[zp], r_a.at[zp])
+        for further in {2: (1, 2), 6: (7,)}.get(d, ()):
+            put(t_all.at[zp], t_all.at[zp], r_a.at[zp], (y, x, lax.rem(z + further, 8), c))
         yd, side = zp // 2, lax.rem(zp, 2)
         xd = 2 * side + c
         rows = t_all[zp]

time: 99.8 us -> 97.9 us (0.981)
  Pallas kernels: 97 us -> 95.5 us
    pallas_call x1, Pallas kernels: 97 us -> 95.5 us  [per_device(): pl.pallas_call(kernel, out_shape=jax.ShapeDtypeStruct((64, 256), B16), in...]
where the time goes in v6:
time: 97.9 us; the launch traced here: 96.9 us
  Pallas kernels  95.5 us (98%)
  local copies, waits for them, and re-layouts  1.38 us (1%)
    pallas_call x1, Pallas kernels, per_device(): pl.pallas_call(kernel, out_shape=jax.ShapeDtypeStruct((64, 256), B16), in...  95.5 us

profile of v6, /device:TPU:2, one launch (start us, length us, event | category | flops | bytes accessed | tf_op | source)
XLA Modules:
  0.0 96.9 jit_solution(13876855512158489426)
XLA Ops:
  0.0 95.5 %layer.1 = bf16[64,256]{1,0:T(8,128)(2,1)} custom-call(bf16[64,256]{1,0:T(8,128)(2,1)} %tok_h.1, s32[1,64]{1,0:T(1,128)} %bitcast.6, f32[1,128]{1,0:T(1,128)} %bitcast.7, f32[1,256]{1,0:T(1,128)} %bitcast.4, f32[1,256]{1,0:T(1,128)} %bitcast.5, f32[2]{0:T(128)} %rates.1, f32[64,64,128]{2,1,0:T(8,128)} %state_h.1, bf16[64,128,128]{2,1,0:T(8,128)(2,1)} %keys_h.1, ...), custom_call_target="tpu_custom_call" | custom-call | tf_op jit(solution)/shard_map/layer/pallas_call | solution.py:700
  95.6 1.4 %copy.18 = bf16[64,256]{1,0:T(8,128)(2,1)} copy(bf16[64,256]{1,0:T(8,128)(2,1)} %layer.1) | data formatting | bytes 65536

commit v7 on v6

--- a/solution.py
+++ b/solution.py
@@ -314,15 +314,6 @@
 
     here[6].wait()
     to_partner(1)
-    for i in (2, 3):
-        arrived(theirs[i], r_w.at[i])
-    gain_rows = jnp.broadcast_to(mixer_gain[...], (8, 256))
-    for half in range(2):
-        col_out[:, pl.ds(1024 * half, 1024)] = split_dot(gain_rows, wu[row_of, half], 3)[0:1]
-    col_in[kv] = col_out[...]
-    for k in (5, 7, 13, 15, 6, 14, 9, 11, 10, 1, 4, 3, 12, 2, 8):
-        to = (lax.rem(y + k // 4, 4), lax.rem(x + k % 4, 4), z, c)
-        put(col_out, col_in.at[kv], r_col.at[0], to)
 
     arrived(b2_in.at[pl.ds(0, 3)], r_b2.at[0], owner)
     arrived(b2_in, r_b2.at[0], jnp.logical_not(owner))
@@ -406,6 +397,17 @@
         d_out[i] = part
         put(d_out.at[i], d_in.at[z], r_d.at[0], (y, x, i, c), jnp.logical_not(mine))
     on_to_sibling(1)
+
+    for i in (2, 3):
+        arrived(theirs[i], r_w.at[i])
+    gain_rows = jnp.broadcast_to(mixer_gain[...], (8, 256))
+    for half in range(2):
+        col_out[:, pl.ds(1024 * half, 1024)] = split_dot(gain_rows, wu[row_of, half], 3)[0:1]
+    col_in[kv] = col_out[...]
+    for k in (5, 7, 13, 15, 6, 14, 9, 11, 10, 1, 4, 3, 12, 2, 8):
+        to = (lax.rem(y + k // 4, 4), lax.rem(x + k % 4, 4), z, c)
+        put(col_out, col_in.at[kv], r_col.at[0], to)
+
     arrived(d_in.at[pl.ds(0, 7)], r_d.at[0])
     branch = d_in[z].astype(F32)
     for d in NEAR[1:]:

time: 97.9 us -> 95.5 us (0.975)
  Pallas kernels: 95.5 us -> 94 us
    pallas_call x1, Pallas kernels: 95.5 us -> 94 us  [per_device(): pl.pallas_call(kernel, out_shape=jax.ShapeDtypeStruct((64, 256), B16), in...]
where the time goes in v7:
time: 95.5 us; the launch traced here: 95.3 us
  Pallas kernels  94 us (98%)
  local copies, waits for them, and re-layouts  1.38 us (1%)
    pallas_call x1, Pallas kernels, per_device(): pl.pallas_call(kernel, out_shape=jax.ShapeDtypeStruct((64, 256), B16), in...  94 us

profile of v7, /device:TPU:2, one launch (start us, length us, event | category | flops | bytes accessed | tf_op | source)
XLA Modules:
  0.0 95.3 jit_solution(7692926575784417087)
XLA Ops:
  0.0 94.0 %layer.1 = bf16[64,256]{1,0:T(8,128)(2,1)} custom-call(bf16[64,256]{1,0:T(8,128)(2,1)} %tok_h.1, s32[1,64]{1,0:T(1,128)} %bitcast.6, f32[1,128]{1,0:T(1,128)} %bitcast.7, f32[1,256]{1,0:T(1,128)} %bitcast.4, f32[1,256]{1,0:T(1,128)} %bitcast.5, f32[2]{0:T(128)} %rates.1, f32[64,64,128]{2,1,0:T(8,128)} %state_h.1, bf16[64,128,128]{2,1,0:T(8,128)(2,1)} %keys_h.1, ...), custom_call_target="tpu_custom_call" | custom-call | tf_op jit(solution)/shard_map/layer/pallas_call | solution.py:702
  94.0 1.4 %copy.18 = bf16[64,256]{1,0:T(8,128)(2,1)} copy(bf16[64,256]{1,0:T(8,128)(2,1)} %layer.1) | data formatting | bytes 65536
